TPU v7x, 512 devices: a 4x2x32 block of a 4x8x32 slice. The times are simulated.
512 devices in a mesh: grp: 2 (over y), kv: 32 (over z), tp: 8 (over x, core).
Axes of the slice: x: 4, y: 2, z: 32, core: 2. Of those that a mesh axis runs over, the one named last changes fastest.
The devices are a block of a 4x8x32 slice.
Arguments:
- tokens: bfloat16 [256, 4096], P('grp', ('kv', 'tp')), parts along dimension 0, may hold values from -50 to 50
- mix_gain: bfloat16 [4096], P('kv'), may hold values from 0.099609375 to 1.8984375
- w_query: bfloat16 [4096, 2048], P('kv', 'tp'), may hold values from -0.09375 to 0.09375
- w_forget: bfloat16 [4096, 2048], P('kv', 'tp'), may hold values from -0.09375 to 0.09375
- w_input: bfloat16 [4096, 2048], P('kv', 'tp'), may hold values from -0.09375 to 0.09375
- w_outgate: bfloat16 [4096, 2048], P('kv', 'tp'), may hold values from -0.09375 to 0.09375
- lower_bound: float32 [2048], P('tp'), may hold values from 0.05 to 0.9
- state: float32 [256, 16, 128, 128], P(('grp', 'kv'), 'tp'), parts along dimension 0, may hold values from -4 to 4
- head_gain: bfloat16 [128], replicated, may hold values from 0.099609375 to 1.8984375
- w_mixout: bfloat16 [2048, 4096], P('tp', 'kv'), may hold values from -0.125 to 0.125
- ffn_gain: bfloat16 [4096], P('kv'), may hold values from 0.099609375 to 1.8984375
- w_gate: bfloat16 [4096, 11264], P('kv', 'tp'), may hold values from -0.09375 to 0.09375
- w_up: bfloat16 [4096, 11264], P('kv', 'tp'), may hold values from -0.09375 to 0.09375
- w_down: bfloat16 [11264, 4096], P('tp', 'kv'), may hold values from -0.0546875 to 0.0546875
Outputs:
- mixed: bfloat16 [256, 4096], P('grp', ('kv', 'tp')), parts along dimension 0
- new_state: float32 [256, 16, 128, 128], P(('grp', 'kv'), 'tp'), parts along dimension 0
There are 2 independent parts, one for each index of `grp`. A program takes and returns all parts, laid end to end along the dimension named above; an argument that names none is the same for every part. Nothing has to cross between parts.
All inputs are finite; a program needn't handle non-finite values.
Results may differ from a plain program's by a relative error of at most 0.01.
Values may be sent and summed in bfloat16 or wider, within the bound.
No kernel may reach another device: no remote copies, remote signals or barrier semaphores. Data moves between devices by JAX's collectives and lax.ppermute only.
A program may use at most 64 MiB of HBM per device.

v0:
```python
import jax
import jax.numpy as jnp
from jax import lax
from jax.sharding import PartitionSpec as P

D = 4096


eps = 0.1


def in_order(parts, dim):
    shape = list(parts.shape[1:])
    shape[dim] *= parts.shape[0]
    return jnp.moveaxis(parts, 0, dim).reshape(shape)


def copy_for_each(array, axis):
    size = lax.axis_size(axis)
    return lax.all_to_all(
        jnp.broadcast_to(array[None], (size, *array.shape)), axis, 0, 0, tiled=True
    )


def gather_directly(array, axis, dim):
    return in_order(copy_for_each(array, axis), dim)


def cut_along(array, dim, size):
    before, after = (array.shape[:dim], array.shape[dim + 1 :])
    return jnp.moveaxis(array.reshape(*before, size, -1, *after), dim, 0)


def summed_on_arrival(array, axis, dim):
    size = lax.axis_size(axis)
    parts = lax.all_to_all(cut_along(array, dim, size), axis, 0, 0, tiled=True)
    return jnp.sum(parts, axis=0)


def in_one_piece(arrays, axis, dim, along):
    columns = [a.reshape(*a.shape[:along], -1) for a in arrays]
    both = jnp.concatenate(columns, axis=along)
    out, at, gathered = (summed_on_arrival(both, axis, dim), 0, [])
    for a, column in zip(arrays, columns):
        piece = out[..., at : at + column.shape[along]]
        gathered.append(piece.reshape(*piece.shape[:along], *a.shape[along:]))
        at += column.shape[along]
    return tuple(gathered)


def over_copies(array, axis):
    return copy_for_each(array, axis).sum(axis=0)


def sum_packed(arrays, axis, dims):
    size = lax.axis_size(axis)
    parts = [cut_along(a, dim, size) for a, dim in zip(arrays, dims)]
    lines = jnp.concatenate([b.reshape(size, -1) for b in parts], axis=1)
    span = max(16, -(-lines.shape[1] // 1024) * 8)
    lines = jnp.pad(lines, ((0, 0), (0, span * 128 - lines.shape[1]))).reshape(-1, 128)
    vector, at, gathered = (lax.psum_scatter(lines, axis, tiled=True).reshape(-1), 0, [])
    for b in parts:
        part = b[0]
        gathered.append(vector[at : at + part.size].reshape(part.shape))
        at += part.size
    return tuple(gathered)


def activate(gate_part, up_part, square_sum):
    inv_rms = lax.rsqrt(square_sum / D + eps)[:, None]
    return (jax.nn.silu(gate_part * inv_rms) * (up_part * inv_rms)).astype(jnp.bfloat16)


def body(
    tokens,
    mix_gain,
    w_query,
    w_forget,
    w_input,
    w_outgate,
    lower_bound,
    state,
    head_gain,
    w_mixout,
    ffn_gain,
    w_gate,
    w_up,
    w_down,
):
    rows_here = state.shape[0]
    heads_here = state.shape[1]
    head_size = state.shape[2]
    token_block = gather_directly(tokens, "tp", 1)
    block_f = token_block.astype(jnp.float32)
    normed = (block_f * mix_gain.astype(jnp.float32)).astype(jnp.bfloat16)
    squares = jnp.sum(block_f * block_f, axis=1)
    query_part = jnp.dot(normed, w_query, preferred_element_type=jnp.float32)
    forget_part = jnp.dot(normed, w_forget, preferred_element_type=jnp.float32)
    input_part = jnp.dot(normed, w_input, preferred_element_type=jnp.float32)
    gate_part = jnp.dot(normed, w_outgate, preferred_element_type=jnp.float32)
    query_raw, forget_raw, input_raw, gate_raw, square_sum = in_one_piece(
        (query_part, forget_part, input_part, gate_part, squares), "kv", 0, 1
    )
    inv_rms = lax.rsqrt(square_sum / D + eps)[:, None]

    def heads_of(values_raw):
        return (values_raw * inv_rms).reshape(rows_here, heads_here, head_size)

    query_act = jax.nn.silu(heads_of(query_raw))
    forget_pre = heads_of(forget_raw)
    values_in = heads_of(input_raw)
    bounds = lower_bound.reshape(heads_here, head_size)
    forget = bounds + (1.0 - bounds) * jax.nn.sigmoid(forget_pre)
    key_in = (1.0 - bounds) * jax.nn.sigmoid(-forget_pre)
    new_state = forget[..., None] * state + key_in[..., None] * values_in[:, :, None, :]
    readout = jnp.sum(query_act[..., None] * new_state, axis=2)
    head_rms = lax.rsqrt(jnp.mean(readout * readout, axis=-1, keepdims=True) + eps)
    gated_out = readout * head_rms * head_gain.astype(jnp.float32) * jax.nn.silu(heads_of(gate_raw))
    gated_out = gated_out.reshape(rows_here, heads_here * head_size).astype(jnp.bfloat16)
    mix_terms = jnp.dot(
        gather_directly(gated_out, "kv", 0), w_mixout, preferred_element_type=jnp.float32
    )
    own_width = tokens.shape[1]
    mix_whole = over_copies(mix_terms, "tp")
    resid_block = (block_f + mix_whole).astype(jnp.bfloat16)
    resid_own = lax.dynamic_slice_in_dim(
        resid_block, lax.axis_index("tp") * own_width, own_width, 1
    )
    resid_f = resid_block.astype(jnp.float32)
    normed_ffn = (resid_f * ffn_gain.astype(jnp.float32)).astype(jnp.bfloat16)
    squares_ffn = jnp.sum(resid_f * resid_f, axis=1)
    gate_terms = jnp.dot(normed_ffn, w_gate, preferred_element_type=jnp.float32)
    up_terms = jnp.dot(normed_ffn, w_up, preferred_element_type=jnp.float32)
    gate_rows, up_rows, square_rows = sum_packed(
        (gate_terms, up_terms, squares_ffn), "kv", (0, 0, 0)
    )
    hidden_rows = activate(gate_rows, up_rows, square_rows)
    down_terms = jnp.dot(
        gather_directly(hidden_rows, "kv", 0), w_down, preferred_element_type=jnp.float32
    )
    down_own = summed_on_arrival(down_terms, "tp", 1)
    mixed = (resid_own.astype(jnp.float32) + down_own).astype(jnp.bfloat16)
    return (mixed, new_state)


def solution(mesh):
    return jax.shard_map(
        body,
        mesh=mesh,
        in_specs=(
            P("grp", ("kv", "tp")),
            P("kv"),
            P("kv", "tp"),
            P("kv", "tp"),
            P("kv", "tp"),
            P("kv", "tp"),
            P("tp"),
            P(("grp", "kv"), "tp", None, None),
            P(),
            P("tp", "kv"),
            P("kv"),
            P("kv", "tp"),
            P("kv", "tp"),
            P("tp", "kv"),
        ),
        out_specs=(P("grp", ("kv", "tp")), P(("grp", "kv"), "tp", None, None)),
        check_vma=False,
    )
```

profile of v0, /device:TPU:33, one launch (start us, length us, event | category | flops | bytes accessed | tf_op | source)
XLA Modules:
  0.0 377.3 jit_solution(3564544453811660452)
XLA Ops:
  7.2 0.0 copy-start
  7.2 0.0 copy-start.4
  7.2 1.4 broadcast_in_dim.8
  8.6 44.7 %all-to-all-start = ((bf16[8,128,16]{1,2,0:T(8,128)(2,1)}), bf16[8,128,16]{1,2,0:T(8,128)(2,1)S(1)}, u32[]{:S(2)}, u32[]{:S(2)}) async-start(bf16[8,128,16]{1,2,0:T(8,128)(2,1)} %broadcast_in_dim.8), calls=%async_computation | async-start | bytes 65536 | tf_op jit(solution)/shard_map/all_to_all | solution.py:20
  53.3 0.7 convert_element_type.78
  53.9 4.1 %all-to-all-done = bf16[8,128,16]{1,2,0:T(8,128)(2,1)S(1)} async-done(((bf16[8,128,16]{1,2,0:T(8,128)(2,1)}), bf16[8,128,16]{1,2,0:T(8,128)(2,1)S(1)}, u32[]{:S(2)}, u32[]{:S(2)}) %all-to-all-start) | async-done | bytes 32800 | tf_op jit(solution)/shard_map/all_to_all | solution.py:20
  58.1 0.2 copy.94
  58.3 0.2 reshape.189
  58.6 0.1 concatenate.9
  58.7 0.3 copy.96
  59.0 0.0 copy-done.4
  59.0 0.1 convolution_dynamic-update-slice_fusion.3
  59.2 0.0 copy-start.10
  59.2 0.0 copy-start.9
  59.2 0.1 convolution_dynamic-update-slice_fusion.2
  59.4 0.1 convolution_dynamic-update-slice_fusion.1
  59.5 0.1 convolution_dynamic-update-slice_fusion
  59.7 0.0 copy-start.1
  59.7 1.2 copy.97
  60.9 6.9 %all-to-all-start.1 = ((f32[32,4,1025]{2,1,0:T(4,128)}), f32[32,4,1025]{2,1,0:T(4,128)S(1)}, u32[]{:S(2)}, u32[]{:S(2)}) async-start(f32[32,4,1025]{2,1,0:T(4,128)} %copy.97), calls=%async_computation.1 | async-start | bytes 1179648 | tf_op jit(solution)/shard_map/all_to_all | solution.py:36
  67.8 0.0 copy-done.10
  67.8 0.0 copy-done.9
  67.8 69.6 %all-to-all-done.1 = f32[32,4,1025]{2,1,0:T(4,128)S(1)} async-done(((f32[32,4,1025]{2,1,0:T(4,128)}), f32[32,4,1025]{2,1,0:T(4,128)S(1)}, u32[]{:S(2)}, u32[]{:S(2)}) %all-to-all-start.1) | async-done | bytes 524832 | tf_op jit(solution)/shard_map/all_to_all | solution.py:36
  137.4 0.1 reduce_sum.66
  137.5 0.1 fusion.13
  137.7 0.1 add_divide_fusion.1
  137.8 0.0 copy-done.1
  137.8 0.0 copy-start.11
  137.9 1.3 multiply_reduce_fusion
  139.1 0.1 multiply_reduce_fusion.3
  139.2 0.1 multiply_bitcast_fusion
  139.3 0.1 fusion.10
  139.4 27.4 %all_to_all.30 = bf16[32,4,256]{2,1,0:T(4,128)(2,1)S(1)} all-to-all(bf16[32,4,256]{2,1,0:T(4,128)(2,1)S(1)} %broadcast_in_dim.9), channel_id=1, replica_groups=mesh['grp'=2,'kv'=32,'tp'=8] {'kv'}, dimensions={0} | all-to-all | bytes 131072 | tf_op jit(solution)/shard_map/all_to_all | solution.py:20
  166.9 0.1 fusion.18
  167.0 0.8 broadcast_in_dim.10
  167.9 6.0 %all-to-all-start.3 = ((f32[8,128,128]{2,1,0:T(8,128)}), f32[8,128,128]{2,1,0:T(8,128)S(1)}, u32[]{:S(2)}, u32[]{:S(2)}) async-start(f32[8,128,128]{2,1,0:T(8,128)} %broadcast_in_dim.10), calls=%async_computation.3 | async-start | bytes 1048576 | tf_op jit(solution)/shard_map/all_to_all | solution.py:20
  173.8 0.1 copy.99
  173.9 9.3 %all-to-all-done.3 = f32[8,128,128]{2,1,0:T(8,128)S(1)} async-done(((f32[8,128,128]{2,1,0:T(8,128)}), f32[8,128,128]{2,1,0:T(8,128)S(1)}, u32[]{:S(2)}, u32[]{:S(2)}) %all-to-all-start.3) | async-done | bytes 524320 | tf_op jit(solution)/shard_map/all_to_all | solution.py:20
  183.3 0.0 copy-start.3
  183.3 0.1 copy.100
  183.4 0.2 fusion.6
  183.7 0.1 reshape_reshape.6
  183.8 0.5 copy-done.3
  184.3 0.2 fusion.5
  184.5 0.1 reshape_reshape.7
  184.7 0.1 reshape.182
  184.8 0.1 select_maximum_fusion
  184.9 1.4 reshape.183
  186.3 0.1 reduce-scatter.2.cloned.1.call-update
  186.4 94.1 %reduce-scatter.2.cloned.1.call-done = f32[96,128]{1,0:T(8,128)} async-done(((f32[3072,128]{1,0:T(8,128)}), f32[96,128]{1,0:T(8,128)}) %reduce-scatter.2.cloned.1.call-update) | async-done | bytes 49168 | tf_op jit(solution)/shard_map/reduce_scatter | solution.py:61
  280.4 0.8 fusion.16
  281.3 0.7 fusion.15
  282.0 0.1 fusion.8
  282.1 0.8 broadcast_in_dim.11
  282.9 16.2 %all-to-all-start.4 = ((bf16[32,4,1408]{2,1,0:T(4,128)(2,1)}), bf16[32,4,1408]{2,1,0:T(4,128)(2,1)S(1)}, u32[]{:S(2)}, u32[]{:S(2)}) async-start(bf16[32,4,1408]{2,1,0:T(4,128)(2,1)} %broadcast_in_dim.11), calls=%async_computation.5 | async-start | bytes 720896 | tf_op jit(solution)/shard_map/all_to_all | solution.py:20
  299.2 0.2 copy.101
  299.4 35.0 %all-to-all-done.4 = bf16[32,4,1408]{2,1,0:T(4,128)(2,1)S(1)} async-done(((bf16[32,4,1408]{2,1,0:T(4,128)(2,1)}), bf16[32,4,1408]{2,1,0:T(4,128)(2,1)S(1)}, u32[]{:S(2)}, u32[]{:S(2)}) %all-to-all-start.4) | async-done | bytes 360480 | tf_op jit(solution)/shard_map/all_to_all | solution.py:20
  334.4 0.1 reshape.194
  334.5 0.9 convolution_bitcast_fusion
  335.4 29.3 %all-to-all-start.5 = ((f32[8,128,16]{1,2,0:T(8,128)}), f32[8,128,16]{1,2,0:T(8,128)S(1)}, u32[]{:S(2)}, u32[]{:S(2)}) async-start(f32[8,128,16]{1,2,0:T(8,128)} %convolution_bitcast_fusion), calls=%async_computation.6 | async-start | bytes 131072 | tf_op jit(solution)/shard_map/all_to_all | solution.py:36
  364.7 4.9 %all-to-all-done.5 = f32[8,128,16]{1,2,0:T(8,128)S(1)} async-done(((f32[8,128,16]{1,2,0:T(8,128)}), f32[8,128,16]{1,2,0:T(8,128)S(1)}, u32[]{:S(2)}, u32[]{:S(2)}) %all-to-all-start.5) | async-done | bytes 65568 | tf_op jit(solution)/shard_map/all_to_all | solution.py:36
  369.6 0.1 copy.102
  369.7 0.1 add_convert_fusion
  369.7 0.7 copy.103
  (35 shorter events, 0.4 us)
Async XLA Ops:
  7.2 176.2 %copy-start = (bf16[128,1408]{1,0:T(8,128)(2,1)S(1)}, bf16[128,1408]{1,0:T(8,128)(2,1)}, u32[]{:S(2)}) copy-start(bf16[128,1408]{1,0:T(8,128)(2,1)} %param.25) | copy-start | bytes 1081348
  7.2 51.8 %copy-start.4 = (bf16[128,256]{1,0:T(8,128)(2,1)S(1)}, bf16[128,256]{1,0:T(8,128)(2,1)}, u32[]{:S(2)}) copy-start(bf16[128,256]{1,0:T(8,128)(2,1)} %param.16) | copy-start | bytes 196612
  7.2 52.0 %copy-start.5 = (bf16[128,256]{1,0:T(8,128)(2,1)S(1)}, bf16[128,256]{1,0:T(8,128)(2,1)}, u32[]{:S(2)}) copy-start(bf16[128,256]{1,0:T(8,128)(2,1)} %param.17) | copy-start | bytes 196612
  7.2 52.1 %copy-start.6 = (bf16[128,256]{1,0:T(8,128)(2,1)S(1)}, bf16[128,256]{1,0:T(8,128)(2,1)}, u32[]{:S(2)}) copy-start(bf16[128,256]{1,0:T(8,128)(2,1)} %param.18) | copy-start | bytes 196612
  7.2 52.3 %copy-start.7 = (bf16[128,256]{1,0:T(8,128)(2,1)S(1)}, bf16[128,256]{1,0:T(8,128)(2,1)}, u32[]{:S(2)}) copy-start(bf16[128,256]{1,0:T(8,128)(2,1)} %param.19) | copy-start | bytes 196612
  8.6 49.5 %all-to-all-start = ((bf16[8,128,16]{1,2,0:T(8,128)(2,1)}), bf16[8,128,16]{1,2,0:T(8,128)(2,1)S(1)}, u32[]{:S(2)}, u32[]{:S(2)}) async-start(bf16[8,128,16]{1,2,0:T(8,128)(2,1)} %broadcast_in_dim.8), calls=%async_computation | async-start | bytes 65536 | tf_op jit(solution)/shard_map/all_to_all | solution.py:20
  59.2 8.6 %copy-start.10 = (bf16[128]{0:T(256)(128)(2,1)S(1)}, bf16[128]{0:T(256)(128)(2,1)}, u32[]{:S(2)}) copy-start(bf16[128]{0:T(256)(128)(2,1)} %param.22) | copy-start | bytes 772
  59.2 8.6 %copy-start.9 = (f32[256]{0:T(256)S(1)}, f32[256]{0:T(256)}, u32[]{:S(2)}) copy-start(f32[256]{0:T(256)} %param.20) | copy-start | bytes 3076
  59.7 78.2 %copy-start.1 = (f32[4,2,128,128]{3,2,1,0:T(8,128)S(1)}, f32[4,2,128,128]{3,2,1,0:T(8,128)}, u32[]{:S(2)}) copy-start(f32[4,2,128,128]{3,2,1,0:T(8,128)} %param.21) | copy-start | bytes 1572868
  60.9 106.0 %copy-start.8 = (bf16[256,128]{1,0:T(8,128)(2,1)S(1)}, bf16[256,128]{1,0:T(8,128)(2,1)}, u32[]{:S(2)}) copy-start(bf16[256,128]{1,0:T(8,128)(2,1)} %param.23) | copy-start | bytes 196612
  60.9 76.5 %all-to-all-start.1 = ((f32[32,4,1025]{2,1,0:T(4,128)}), f32[32,4,1025]{2,1,0:T(4,128)S(1)}, u32[]{:S(2)}, u32[]{:S(2)}) async-start(f32[32,4,1025]{2,1,0:T(4,128)} %copy.97), calls=%async_computation.1 | async-start | bytes 1179648 | tf_op jit(solution)/shard_map/all_to_all | solution.py:36
  137.8 36.0 %copy-start.11 = (bf16[128]{0:T(256)(128)(2,1)S(1)}, bf16[128]{0:T(256)(128)(2,1)}, u32[]{:S(2)}) copy-start(bf16[128]{0:T(256)(128)(2,1)} %param.24) | copy-start | bytes 772
  167.9 15.4 %all-to-all-start.3 = ((f32[8,128,128]{2,1,0:T(8,128)}), f32[8,128,128]{2,1,0:T(8,128)S(1)}, u32[]{:S(2)}, u32[]{:S(2)}) async-start(f32[8,128,128]{2,1,0:T(8,128)} %broadcast_in_dim.10), calls=%async_computation.3 | async-start | bytes 1048576 | tf_op jit(solution)/shard_map/all_to_all | solution.py:20
  173.8 106.6 %reduce-scatter.2.cloned.1.call-start = ((), (), s32[]{:S(2)}) async-start(), calls=%async_computation.7 | async-start | bytes 1622016 | tf_op jit(solution)/shard_map/reduce_scatter | solution.py:61
  183.3 1.0 copy-start.3
  186.3 112.9 %copy-start.2 = (bf16[1408,128]{1,0:T(8,128)(2,1)S(1)}, bf16[1408,128]{1,0:T(8,128)(2,1)}, u32[]{:S(2)}) copy-start(bf16[1408,128]{1,0:T(8,128)(2,1)} %param.27) | copy-start | bytes 1081348
  282.9 51.5 %all-to-all-start.4 = ((bf16[32,4,1408]{2,1,0:T(4,128)(2,1)}), bf16[32,4,1408]{2,1,0:T(4,128)(2,1)S(1)}, u32[]{:S(2)}, u32[]{:S(2)}) async-start(bf16[32,4,1408]{2,1,0:T(4,128)(2,1)} %broadcast_in_dim.11), calls=%async_computation.5 | async-start | bytes 720896 | tf_op jit(solution)/shard_map/all_to_all | solution.py:20
  335.4 34.2 %all-to-all-start.5 = ((f32[8,128,16]{1,2,0:T(8,128)}), f32[8,128,16]{1,2,0:T(8,128)S(1)}, u32[]{:S(2)}, u32[]{:S(2)}) async-start(f32[8,128,16]{1,2,0:T(8,128)} %convolution_bitcast_fusion), calls=%async_computation.6 | async-start | bytes 131072 | tf_op jit(solution)/shard_map/all_to_all | solution.py:36
Sparse Core Ops, SparseCore 0:
  186.5 93.9 reduce-scatter.1
where the time goes:
time: 378 us; the launch traced here: 377 us
  waiting for transfers between devices  217 us (57%)
  starting transfers between devices  103 us (27%)
  blocking collectives  27.4 us (7%)
  between operations  14.5 us (4%)
  local copies, waits for them, and re-layouts  9.56 us (3%)
    reduce_scatter x1, waiting for transfers between devices, sum_packed(): lax.psum_scatter(lines, axis, tiled=True).reshape(-1)  94.1 us
    all_to_all x2, waiting for transfers between devices, summed_on_arrival(): parts = lax.all_to_all(cut_along(array, dim, size), axis, 0, 0, tiled=True)  74.5 us
    all_to_all x3, starting transfers between devices, copy_for_each(): lax.all_to_all(jnp.broadcast_to(array[None], (size, *array.shape)), axis,...  66.9 us
    all_to_all x3, waiting for transfers between devices, copy_for_each(): lax.all_to_all(jnp.broadcast_to(array[None], (size, *array.shape)), axis,...  48.5 us
    all_to_all x2, starting transfers between devices, summed_on_arrival(): parts = lax.all_to_all(cut_along(array, dim, size), axis, 0, 0, tiled=True)  36.2 us
    all_to_all x1, blocking collectives, copy_for_each(): lax.all_to_all(jnp.broadcast_to(array[None], (size, *array.shape)), axis,...  27.4 us
  transfers between devices with their start and end apart: 6, of which 6 were waited for; matrix products, arithmetic and copies ran while one was open for 0% of the time, Pallas kernels for 0%

commit v1 on v0

v1 whole, which is shorter than its diff:
```python
import jax
import jax.numpy as jnp
from jax import lax
from jax.sharding import PartitionSpec as P

D = 4096
NEAR = 4

eps = 0.1
bf16, f32 = jnp.bfloat16, jnp.float32


def spread(parts, axis, groups=None):
    return lax.all_to_all(parts, axis, 0, 0, axis_index_groups=groups, tiled=True)


def share(array, axis, size, groups=None):
    return spread(jnp.broadcast_to(array[None], (size, *array.shape)), axis, groups)


def summed(parts):
    return jnp.sum(parts.astype(f32), axis=0)


def dot_t(left, right, contract):
    return lax.dot_general(left, right, (contract, ((), ())), preferred_element_type=f32)


def pick(stack, index):
    return lax.dynamic_index_in_dim(stack, index, 0, keepdims=False)


def exchanged(stack, place, groups):
    got = [pick(stack, place)]
    for k in range(1, NEAR):
        pairs = [(g[i], g[i ^ k]) for g in groups for i in range(NEAR)]
        got.append(lax.ppermute(pick(stack, place ^ k), "kv", pairs))
    got = jnp.stack(got)
    return jnp.stack([pick(got, j ^ place) for j in range(NEAR)])


def body(
    tokens,
    mix_gain,
    w_query,
    w_forget,
    w_input,
    w_outgate,
    lower_bound,
    state,
    head_gain,
    w_mixout,
    ffn_gain,
    w_gate,
    w_up,
    w_down,
):
    rows_here, heads_here, head_size = state.shape[:3]
    kv, tp = lax.axis_size("kv"), lax.axis_size("tp")
    batch, own_width = tokens.shape
    far = kv // NEAR
    near_groups = [[NEAR * a + b for b in range(NEAR)] for a in range(far)]
    far_groups = [[NEAR * a + b for a in range(far)] for b in range(NEAR)]
    block_groups = [
        [(NEAR * a + b) * tp + t for b in range(NEAR) for t in range(tp)] for a in range(far)
    ]
    place = lax.axis_index("kv") % NEAR

    units = w_gate.shape[1] // NEAR
    width = -(-(2 * units + 1) // 128) * 128
    pad = jnp.zeros((w_gate.shape[0], width - 2 * units - 1), bf16)
    cut = lambda w, j: w[:, j * units : (j + 1) * units]
    pieces = jnp.stack(
        [
            jnp.concatenate([cut(w_gate, j), cut(w_up, j), ffn_gain[:, None], pad], axis=1)
            for j in range(NEAR)
        ]
    )
    w_gate_up = exchanged(pieces, place, near_groups).reshape(-1, width)
    w_out = exchanged(w_down.reshape(NEAR, units, -1), place, near_groups)

    block = share(tokens.T, "tp", tp).reshape(-1, batch)
    block_f = block.astype(f32)
    normed = (block_f * mix_gain.astype(f32)[:, None]).astype(bf16)
    squares = jnp.sum(block_f * block_f, axis=0)
    weights = (w_query, w_forget, w_input, w_outgate)
    terms = [dot_t(normed, w, ((0,), (0,))).astype(bf16) for w in weights]
    side = jnp.broadcast_to(squares.astype(bf16)[:, None], (batch, 128))
    terms = jnp.concatenate(terms + [side], axis=1)
    terms = terms.reshape(far, NEAR, rows_here, -1).transpose(1, 0, 2, 3)
    terms = summed(spread(terms, "kv", near_groups)).astype(bf16)
    sums = summed(spread(terms, "kv", far_groups))
    key_width = heads_here * head_size
    inv_rms = lax.rsqrt(sums[:, 4 * key_width : 4 * key_width + 1] / D + eps)
    raw = [
        (sums[:, i * key_width : (i + 1) * key_width] * inv_rms).reshape(
            rows_here, heads_here, head_size
        )
        for i in range(4)
    ]

    query_act = jax.nn.silu(raw[0])
    bounds = lower_bound.reshape(heads_here, head_size)
    forget = bounds + (1.0 - bounds) * jax.nn.sigmoid(raw[1])
    key_in = (1.0 - bounds) * jax.nn.sigmoid(-raw[1])
    new_state = forget[..., None] * state + key_in[..., None] * raw[2][:, :, None, :]
    readout = jnp.sum(query_act[..., None] * new_state, axis=2)
    head_rms = lax.rsqrt(jnp.mean(readout * readout, axis=-1, keepdims=True) + eps)
    gated = readout * head_rms * head_gain.astype(f32) * jax.nn.silu(raw[3])
    gated = gated.reshape(rows_here, key_width).astype(bf16)

    gated_all = share(gated, "kv", kv).reshape(batch, key_width)
    mix = dot_t(w_mixout, gated_all, ((0,), (1,))).astype(bf16)
    resid = (block_f + summed(share(mix, "tp", tp))).astype(bf16)
    resid_own = lax.dynamic_slice_in_dim(resid, lax.axis_index("tp") * own_width, own_width, 0)

    resid_f = share(resid, "kv", NEAR, near_groups).reshape(-1, batch).astype(f32)
    gain = w_gate_up[:, 2 * units : 2 * units + 1].astype(f32)
    normed_ffn = (resid_f * gain).astype(bf16)
    squares_ffn = jnp.sum(resid_f * resid_f, axis=0)
    terms = dot_t(normed_ffn, w_gate_up, ((0,), (0,)))
    column = lax.broadcasted_iota(jnp.int32, terms.shape, 1)
    terms = jnp.where(column == 2 * units, squares_ffn[:, None], terms).astype(bf16)
    sums = summed(spread(terms.reshape(far, -1, width), "kv", far_groups))
    inv_rms = lax.rsqrt(sums[:, 2 * units : 2 * units + 1] / D + eps)
    gate_sum, up_sum = sums[:, :units] * inv_rms, sums[:, units : 2 * units] * inv_rms
    hidden = (jax.nn.silu(gate_sum) * up_sum).astype(bf16)
    hidden_all = share(hidden, "kv", far, far_groups).reshape(batch, units)
    down = dot_t(w_out, hidden_all, ((1,), (1,))).astype(bf16)
    down = summed(spread(down.reshape(NEAR * tp, own_width, batch), ("kv", "tp"), block_groups))
    mixed = (resid_own.astype(f32) + down).astype(bf16).T
    return (mixed, new_state)


def solution(mesh):
    return jax.shard_map(
        body,
        mesh=mesh,
        in_specs=(
            P("grp", ("kv", "tp")),
            P("kv"),
            P("kv", "tp"),
            P("kv", "tp"),
            P("kv", "tp"),
            P("kv", "tp"),
            P("tp"),
            P(("grp", "kv"), "tp", None, None),
            P(),
            P("tp", "kv"),
            P("kv"),
            P("kv", "tp"),
            P("kv", "tp"),
            P("tp", "kv"),
        ),
        out_specs=(P("grp", ("kv", "tp")), P(("grp", "kv"), "tp", None, None)),
        check_vma=False,
    )
```

time: 378 us -> 247 us (0.65)
  waiting for transfers between devices: 217 us -> 81.2 us
  blocking collectives: 27.4 us -> 41.3 us
  between operations: 14.5 us -> 1.09 us
  starting transfers between devices: 103 us -> 107 us
    reduce_scatter x1 -> x0, waiting for transfers between devices: 94.1 us -> none  [sum_packed(): lax.psum_scatter(lines, axis, tiled=True).reshape(-1)]
    all_to_all x5 -> x7, waiting for transfers between devices: 123 us -> 64.6 us  [spread(): lax.all_to_all(parts, axis, 0, 0, axis_index_groups=groups, tiled=True)]
    ppermute x0 -> x6, starting transfers between devices: none -> 18.7 us  [exchanged(): got.append(lax.ppermute(pick(stack, place ^ k), 'kv', pairs))]
    ppermute x0 -> x6, waiting for transfers between devices: none -> 16.6 us  [exchanged(): got.append(lax.ppermute(pick(stack, place ^ k), 'kv', pairs))]
    all_to_all x5 -> x7, starting transfers between devices: 103 us -> 88.2 us  [spread(): lax.all_to_all(parts, axis, 0, 0, axis_index_groups=groups, tiled=True)]
    all_to_all x1 -> x2, blocking collectives: 27.4 us -> 41.3 us  [spread(): lax.all_to_all(parts, axis, 0, 0, axis_index_groups=groups, tiled=True)]
  transfers between devices with their start and end apart: 6 -> 13, of which waited for: 6 -> 8; matrix products, arithmetic and copies ran while one was open for 0% -> 1% of each run, Pallas kernels for 0% -> 0%
where the time goes in v1:
time: 247 us; the launch traced here: 246 us
  starting transfers between devices  107 us (43%)
  waiting for transfers between devices  81.2 us (33%)
  blocking collectives  41.3 us (17%)
  local copies, waits for them, and re-layouts  8.75 us (4%)
  other arithmetic  4.59 us (2%)
    all_to_all x7, starting transfers between devices, spread(): lax.all_to_all(parts, axis, 0, 0, axis_index_groups=groups, tiled=True)  88.2 us
    all_to_all x7, waiting for transfers between devices, spread(): lax.all_to_all(parts, axis, 0, 0, axis_index_groups=groups, tiled=True)  64.6 us
    all_to_all x2, blocking collectives, spread(): lax.all_to_all(parts, axis, 0, 0, axis_index_groups=groups, tiled=True)  41.3 us
    ppermute x6, starting transfers between devices, exchanged(): got.append(lax.ppermute(pick(stack, place ^ k), 'kv', pairs))  18.7 us
    ppermute x6, waiting for transfers between devices, exchanged(): got.append(lax.ppermute(pick(stack, place ^ k), 'kv', pairs))  16.6 us
  transfers between devices with their start and end apart: 13, of which 8 were waited for; matrix products, arithmetic and copies ran while one was open for 1% of the time, Pallas kernels for 0%

profile of v1, /device:TPU:33, one launch (start us, length us, event | category | flops | bytes accessed | tf_op | source)
XLA Modules:
  0.0 246.0 jit_solution(8076468073163946439)
XLA Ops:
  0.6 1.3 broadcast_in_dim.21
  2.0 44.8 %all-to-all-start = ((bf16[8,16,128]{2,1,0:T(8,128)(2,1)}), bf16[8,16,128]{2,1,0:T(8,128)(2,1)S(1)}, u32[]{:S(2)}, u32[]{:S(2)}) async-start(bf16[8,16,128]{2,1,0:T(8,128)(2,1)} %broadcast_in_dim.21), calls=%async_computation | async-start | bytes 65536 | tf_op jit(solution)/shard_map/all_to_all | solution.py:14
  46.8 4.8 %all-to-all-done = bf16[8,16,128]{2,1,0:T(8,128)(2,1)S(1)} async-done(((bf16[8,16,128]{2,1,0:T(8,128)(2,1)}), bf16[8,16,128]{2,1,0:T(8,128)(2,1)S(1)}, u32[]{:S(2)}, u32[]{:S(2)}) %all-to-all-start) | async-done | bytes 32800 | tf_op jit(solution)/shard_map/all_to_all | solution.py:14
  51.6 0.1 fusion.27
  51.7 0.2 fusion.5
  51.9 0.6 copy-done.5
  52.5 0.2 fusion.4
  52.7 0.6 copy-done.6
  53.4 0.2 fusion.3
  53.6 0.6 copy-done.7
  54.2 0.2 fusion.2
  54.4 0.1 broadcast_dynamic-update-slice_fusion
  54.6 0.1 copy.123
  54.7 11.1 %all_to_all.45 = bf16[4,8,4,1152]{3,2,1,0:T(4,128)(2,1)S(1)} all-to-all(bf16[4,8,4,1152]{3,2,1,0:T(4,128)(2,1)S(1)} %bitcast.81), channel_id=1, replica_groups={{0,8,16,24},{32,40,48,56},{64,72,80,88},{96,104,112,120},{128,136,144,1..., dimensions={0} | all-to-all | bytes 589824 | tf_op jit(solution)/shard_map/all_to_all | solution.py:14
  65.9 0.8 reduce_sum.85
  66.6 6.7 %all-to-all-start.2 = ((bf16[8,4,1152]{2,1,0:T(4,128)(2,1)}), bf16[8,4,1152]{2,1,0:T(4,128)(2,1)S(1)}, u32[]{:S(2)}, u32[]{:S(2)}) async-start(bf16[8,4,1152]{2,1,0:T(4,128)(2,1)} %reduce_sum.85), calls=%async_computation.2 | async-start | bytes 147456 | tf_op jit(solution)/shard_map/all_to_all | solution.py:14
  73.4 0.7 copy-done.9
  74.0 23.3 %all-to-all-done.2 = bf16[8,4,1152]{2,1,0:T(4,128)(2,1)S(1)} async-done(((bf16[8,4,1152]{2,1,0:T(4,128)(2,1)}), bf16[8,4,1152]{2,1,0:T(4,128)(2,1)S(1)}, u32[]{:S(2)}, u32[]{:S(2)}) %all-to-all-start.2) | async-done | bytes 73760 | tf_op jit(solution)/shard_map/all_to_all | solution.py:14
  97.4 0.1 fusion.39
  97.5 0.1 add_divide_fusion.1
  97.7 1.3 multiply_reduce_fusion
  99.0 0.1 multiply_reduce_fusion.1
  99.1 0.1 fusion.36
  99.2 0.6 broadcast_in_dim.23
  99.9 4.7 %all-to-all-start.3 = ((bf16[32,4,256]{2,1,0:T(4,128)(2,1)}), bf16[32,4,256]{2,1,0:T(4,128)(2,1)S(1)}, u32[]{:S(2)}, u32[]{:S(2)}) async-start(bf16[32,4,256]{2,1,0:T(4,128)(2,1)} %broadcast_in_dim.23), calls=%async_computation.3 | async-start | bytes 131072 | tf_op jit(solution)/shard_map/all_to_all | solution.py:14
  104.7 0.6 copy-done.10
  105.3 0.1 copy.107
  105.5 0.1 pad.27.clone
  105.5 0.3 fusion.41
  105.8 0.3 fusion.17
  106.2 21.0 %all-to-all-done.3 = bf16[32,4,256]{2,1,0:T(4,128)(2,1)S(1)} async-done(((bf16[32,4,256]{2,1,0:T(4,128)(2,1)}), bf16[32,4,256]{2,1,0:T(4,128)(2,1)S(1)}, u32[]{:S(2)}, u32[]{:S(2)}) %all-to-all-start.3) | async-done | bytes 65568 | tf_op jit(solution)/shard_map/all_to_all | solution.py:14
  127.2 0.1 fusion.6
  127.4 0.1 copy.105
  127.5 0.7 broadcast_in_dim.24
  128.3 7.9 %all-to-all-start.4 = ((bf16[8,128,128]{2,1,0:T(8,128)(2,1)}), bf16[8,128,128]{2,1,0:T(8,128)(2,1)S(1)}, u32[]{:S(2)}, u32[]{:S(2)}) async-start(bf16[8,128,128]{2,1,0:T(8,128)(2,1)} %broadcast_in_dim.24), calls=%async_computation.4 | async-start | bytes 524288 | tf_op jit(solution)/shard_map/all_to_all | solution.py:14
  136.2 0.1 pad_maximum_fusion
  136.3 2.2 collective-permute-start.5
  138.6 3.1 %collective-permute-start.4 = (bf16[128,768]{1,0:T(8,128)(2,1)S(1)}, bf16[128,768]{1,0:T(8,128)(2,1)S(1)}, u32[]{:S(2)}, u32[]{:S(2)}) collective-permute-start(bf16[128,768]{1,0:T(8,128)(2,1)S(1)} %get-tuple-element.10), channel_id=1, source_target_pairs={{0,16},{8,24},{16,0},{24,8},{32,48},{40,56},{48,32},{56,40},{64,80... | collective-permute-start | bytes 589832 | tf_op jit(solution)/shard_map/ppermute | solution.py:37
  141.7 4.1 %collective-permute-start.3 = (bf16[128,768]{1,0:T(8,128)(2,1)S(1)}, bf16[128,768]{1,0:T(8,128)(2,1)S(1)}, u32[]{:S(2)}, u32[]{:S(2)}) collective-permute-start(bf16[128,768]{1,0:T(8,128)(2,1)S(1)} %get-tuple-element.11), channel_id=1, source_target_pairs={{0,8},{8,0},{16,24},{24,16},{32,40},{40,32},{48,56},{56,48},{64,72... | collective-permute-start | bytes 589832 | tf_op jit(solution)/shard_map/ppermute | solution.py:37
  145.8 0.1 copy.106
  145.9 0.7 broadcast_in_dim.25
  146.6 3.4 %all-to-all-start.5 = ((bf16[4,128,128]{1,2,0:T(8,128)(2,1)}), bf16[4,128,128]{1,2,0:T(8,128)(2,1)S(1)}, u32[]{:S(2)}, u32[]{:S(2)}) async-start(bf16[4,128,128]{1,2,0:T(8,128)(2,1)} %broadcast_in_dim.25), calls=%async_computation.5 | async-start | bytes 262144 | tf_op jit(solution)/shard_map/all_to_all | solution.py:14
  150.0 8.4 %collective-permute-done.4 = bf16[128,768]{1,0:T(8,128)(2,1)S(1)} collective-permute-done((bf16[128,768]{1,0:T(8,128)(2,1)S(1)}, bf16[128,768]{1,0:T(8,128)(2,1)S(1)}, u32[]{:S(2)}, u32[]{:S(2)}) %collective-permute-start.4) | collective-permute-done | bytes 196640 | tf_op jit(solution)/shard_map/ppermute | solution.py:37
  158.4 0.1 pad_maximum_fusion.1
  158.6 0.1 pad_maximum_fusion.2
  158.7 0.1 slice_convert_fusion
  158.8 0.1 copy.117
  159.0 0.9 all-to-all-done.5
  159.9 0.1 fusion.14
  160.0 0.3 fusion.1
  160.3 30.2 %all_to_all.46 = bf16[8,16,768]{2,1,0:T(8,128)(2,1)S(1)} all-to-all(bf16[8,16,768]{2,1,0:T(8,128)(2,1)S(1)} %bitcast.82), channel_id=1, replica_groups={{0,32,64,96,128,160,192,224},{8,40,72,104,136,168,200,232},{16,48,80,11..., dimensions={0} | all-to-all | bytes 393216 | tf_op jit(solution)/shard_map/all_to_all | solution.py:14
  190.5 0.2 fusion.33
  190.7 0.1 fusion.30
  190.8 0.6 broadcast_in_dim.29
  191.4 10.2 %all-to-all-start.7 = ((bf16[8,16,352]{2,1,0:T(8,128)(2,1)}), bf16[8,16,352]{2,1,0:T(8,128)(2,1)S(1)}, u32[]{:S(2)}, u32[]{:S(2)}) async-start(bf16[8,16,352]{2,1,0:T(8,128)(2,1)} %broadcast_in_dim.29), calls=%async_computation.7 | async-start | bytes 196608 | tf_op jit(solution)/shard_map/all_to_all | solution.py:14
  201.7 3.9 %collective-permute-start.2 = (bf16[352,128]{1,0:T(8,128)(2,1)S(1)}, bf16[352,128]{1,0:T(8,128)(2,1)S(1)}, u32[]{:S(2)}, u32[]{:S(2)}) collective-permute-start(bf16[352,128]{1,0:T(8,128)(2,1)S(1)} %get-tuple-element.17), channel_id=1, source_target_pairs={{0,24},{8,16},{16,8},{24,0},{32,56},{40,48},{48,40},{56,32},{64,88... | collective-permute-start | bytes 270344 | tf_op jit(solution)/shard_map/ppermute | solution.py:37
  205.6 2.0 collective-permute-start.1
  207.6 3.5 %collective-permute-start = (bf16[352,128]{1,0:T(8,128)(2,1)S(1)}, bf16[352,128]{1,0:T(8,128)(2,1)S(1)}, u32[]{:S(2)}, u32[]{:S(2)}) collective-permute-start(bf16[352,128]{1,0:T(8,128)(2,1)S(1)} %get-tuple-element.19), channel_id=1, source_target_pairs={{0,8},{8,0},{16,24},{24,16},{32,40},{40,32},{48,56},{56,48},{64,72... | collective-permute-start | bytes 270344 | tf_op jit(solution)/shard_map/ppermute | solution.py:37
  211.1 8.2 %collective-permute-done.1 = bf16[352,128]{1,0:T(8,128)(2,1)S(1)} collective-permute-done((bf16[352,128]{1,0:T(8,128)(2,1)S(1)}, bf16[352,128]{1,0:T(8,128)(2,1)S(1)}, u32[]{:S(2)}, u32[]{:S(2)}) %collective-permute-start.1) | collective-permute-done | bytes 90144 | tf_op jit(solution)/shard_map/ppermute | solution.py:37
  219.4 6.2 %all-to-all-done.7 = bf16[8,16,352]{2,1,0:T(8,128)(2,1)S(1)} async-done(((bf16[8,16,352]{2,1,0:T(8,128)(2,1)}), bf16[8,16,352]{2,1,0:T(8,128)(2,1)S(1)}, u32[]{:S(2)}, u32[]{:S(2)}) %all-to-all-start.7) | async-done | bytes 90144 | tf_op jit(solution)/shard_map/all_to_all | solution.py:14
  225.5 0.9 convolution_convert_fusion
  226.5 10.4 %all-to-all-start.8 = ((bf16[32,16,128]{2,1,0:T(8,128)(2,1)}), bf16[32,16,128]{2,1,0:T(8,128)(2,1)S(1)}, u32[]{:S(2)}, u32[]{:S(2)}) async-start(bf16[32,16,128]{2,1,0:T(8,128)(2,1)} %bitcast.30), calls=%async_computation.8 | async-start | bytes 262144 | tf_op jit(solution)/shard_map/all_to_all | solution.py:14
  236.9 8.4 %all-to-all-done.8 = bf16[32,16,128]{2,1,0:T(8,128)(2,1)S(1)} async-done(((bf16[32,16,128]{2,1,0:T(8,128)(2,1)}), bf16[32,16,128]{2,1,0:T(8,128)(2,1)S(1)}, u32[]{:S(2)}, u32[]{:S(2)}) %all-to-all-start.8) | async-done | bytes 131104 | tf_op jit(solution)/shard_map/all_to_all | solution.py:14
  245.4 0.6 fusion.35
  (52 shorter events, 0.8 us)
Async XLA Ops:
  0.6 51.0 %copy-start = (bf16[128,256]{1,0:T(8,128)(2,1)S(1)}, bf16[128,256]{1,0:T(8,128)(2,1)}, u32[]{:S(2)}) copy-start(bf16[128,256]{1,0:T(8,128)(2,1)} %param.16) | copy-start | bytes 196612
  2.0 44.8 %copy-start.11 = (bf16[128]{0:T(256)(128)(2,1)S(1)}, bf16[128]{0:T(256)(128)(2,1)}, u32[]{:S(2)}) copy-start(bf16[128]{0:T(256)(128)(2,1)} %param.15) | copy-start | bytes 772
  2.0 49.6 %all-to-all-start = ((bf16[8,16,128]{2,1,0:T(8,128)(2,1)}), bf16[8,16,128]{2,1,0:T(8,128)(2,1)S(1)}, u32[]{:S(2)}, u32[]{:S(2)}) async-start(bf16[8,16,128]{2,1,0:T(8,128)(2,1)} %broadcast_in_dim.21), calls=%async_computation | async-start | bytes 65536 | tf_op jit(solution)/shard_map/all_to_all | solution.py:14
  51.7 0.8 copy-start.5
  52.5 0.8 copy-start.6
  53.4 0.8 copy-start.7
  54.7 42.9 %copy-start.1 = (f32[4,2,128,128]{3,2,1,0:T(8,128)S(1)}, f32[4,2,128,128]{3,2,1,0:T(8,128)}, u32[]{:S(2)}) copy-start(f32[4,2,128,128]{3,2,1,0:T(8,128)} %param.21) | copy-start | bytes 1572868
  66.6 6.7 %copy-start.12 = (bf16[128]{0:T(256)(128)(2,1)S(1)}, bf16[128]{0:T(256)(128)(2,1)}, u32[]{:S(2)}) copy-start(bf16[128]{0:T(256)(128)(2,1)} %param.22) | copy-start | bytes 772
  66.6 30.7 %all-to-all-start.2 = ((bf16[8,4,1152]{2,1,0:T(4,128)(2,1)}), bf16[8,4,1152]{2,1,0:T(4,128)(2,1)S(1)}, u32[]{:S(2)}, u32[]{:S(2)}) async-start(bf16[8,4,1152]{2,1,0:T(4,128)(2,1)} %reduce_sum.85), calls=%async_computation.2 | async-start | bytes 147456 | tf_op jit(solution)/shard_map/all_to_all | solution.py:14
  73.3 0.7 copy-start.9
  97.7 7.8 %copy-start.2 = (bf16[128,1408]{1,0:T(8,128)(2,1)S(1)}, bf16[128,1408]{1,0:T(8,128)(2,1)}, u32[]{:S(2)}) copy-start(bf16[128,1408]{1,0:T(8,128)(2,1)} %param.25) | copy-start | bytes 1081348
  97.7 7.8 %copy-start.3 = (bf16[128,1408]{1,0:T(8,128)(2,1)S(1)}, bf16[128,1408]{1,0:T(8,128)(2,1)}, u32[]{:S(2)}) copy-start(bf16[128,1408]{1,0:T(8,128)(2,1)} %param.26) | copy-start | bytes 1081348
  99.9 27.3 %all-to-all-start.3 = ((bf16[32,4,256]{2,1,0:T(4,128)(2,1)}), bf16[32,4,256]{2,1,0:T(4,128)(2,1)S(1)}, u32[]{:S(2)}, u32[]{:S(2)}) async-start(bf16[32,4,256]{2,1,0:T(4,128)(2,1)} %broadcast_in_dim.23), calls=%async_computation.3 | async-start | bytes 131072 | tf_op jit(solution)/shard_map/all_to_all | solution.py:14
  104.7 0.7 copy-start.10
  106.2 21.1 %copy-start.8 = (bf16[256,128]{1,0:T(8,128)(2,1)S(1)}, bf16[256,128]{1,0:T(8,128)(2,1)}, u32[]{:S(2)}) copy-start(bf16[256,128]{1,0:T(8,128)(2,1)} %param.23) | copy-start | bytes 196612
  128.3 17.5 %all-to-all-start.4 = ((bf16[8,128,128]{2,1,0:T(8,128)(2,1)}), bf16[8,128,128]{2,1,0:T(8,128)(2,1)S(1)}, u32[]{:S(2)}, u32[]{:S(2)}) async-start(bf16[8,128,128]{2,1,0:T(8,128)(2,1)} %broadcast_in_dim.24), calls=%async_computation.4 | async-start | bytes 524288 | tf_op jit(solution)/shard_map/all_to_all | solution.py:14
  136.3 13.7 %collective-permute-start.5 = (bf16[128,768]{1,0:T(8,128)(2,1)S(1)}, bf16[128,768]{1,0:T(8,128)(2,1)S(1)}, u32[]{:S(2)}, u32[]{:S(2)}) collective-permute-start(bf16[128,768]{1,0:T(8,128)(2,1)S(1)} %get-tuple-element.9), channel_id=1, source_target_pairs={{0,24},{8,16},{16,8},{24,0},{32,56},{40,48},{48,40},{56,32},{64,88... | collective-permute-start | bytes 589832 | tf_op jit(solution)/shard_map/ppermute | solution.py:37
  138.6 19.9 %collective-permute-start.4 = (bf16[128,768]{1,0:T(8,128)(2,1)S(1)}, bf16[128,768]{1,0:T(8,128)(2,1)S(1)}, u32[]{:S(2)}, u32[]{:S(2)}) collective-permute-start(bf16[128,768]{1,0:T(8,128)(2,1)S(1)} %get-tuple-element.10), channel_id=1, source_target_pairs={{0,16},{8,24},{16,0},{24,8},{32,48},{40,56},{48,32},{56,40},{64,80... | collective-permute-start | bytes 589832 | tf_op jit(solution)/shard_map/ppermute | solution.py:37
  141.7 16.8 %collective-permute-start.3 = (bf16[128,768]{1,0:T(8,128)(2,1)S(1)}, bf16[128,768]{1,0:T(8,128)(2,1)S(1)}, u32[]{:S(2)}, u32[]{:S(2)}) collective-permute-start(bf16[128,768]{1,0:T(8,128)(2,1)S(1)} %get-tuple-element.11), channel_id=1, source_target_pairs={{0,8},{8,0},{16,24},{24,16},{32,40},{40,32},{48,56},{56,48},{64,72... | collective-permute-start | bytes 589832 | tf_op jit(solution)/shard_map/ppermute | solution.py:37
  146.6 13.2 %all-to-all-start.5 = ((bf16[4,128,128]{1,2,0:T(8,128)(2,1)}), bf16[4,128,128]{1,2,0:T(8,128)(2,1)S(1)}, u32[]{:S(2)}, u32[]{:S(2)}) async-start(bf16[4,128,128]{1,2,0:T(8,128)(2,1)} %broadcast_in_dim.25), calls=%async_computation.5 | async-start | bytes 262144 | tf_op jit(solution)/shard_map/all_to_all | solution.py:14
  190.4 11.2 %copy-start.4 = (bf16[1408,128]{1,0:T(8,128)(2,1)S(1)}, bf16[1408,128]{1,0:T(8,128)(2,1)}, u32[]{:S(2)}) copy-start(bf16[1408,128]{1,0:T(8,128)(2,1)} %param.27) | copy-start | bytes 1081348
  191.4 34.1 %all-to-all-start.7 = ((bf16[8,16,352]{2,1,0:T(8,128)(2,1)}), bf16[8,16,352]{2,1,0:T(8,128)(2,1)S(1)}, u32[]{:S(2)}, u32[]{:S(2)}) async-start(bf16[8,16,352]{2,1,0:T(8,128)(2,1)} %broadcast_in_dim.29), calls=%async_computation.7 | async-start | bytes 196608 | tf_op jit(solution)/shard_map/all_to_all | solution.py:14
  201.7 9.4 %collective-permute-start.2 = (bf16[352,128]{1,0:T(8,128)(2,1)S(1)}, bf16[352,128]{1,0:T(8,128)(2,1)S(1)}, u32[]{:S(2)}, u32[]{:S(2)}) collective-permute-start(bf16[352,128]{1,0:T(8,128)(2,1)S(1)} %get-tuple-element.17), channel_id=1, source_target_pairs={{0,24},{8,16},{16,8},{24,0},{32,56},{40,48},{48,40},{56,32},{64,88... | collective-permute-start | bytes 270344 | tf_op jit(solution)/shard_map/ppermute | solution.py:37
  205.6 13.6 %collective-permute-start.1 = (bf16[352,128]{1,0:T(8,128)(2,1)S(1)}, bf16[352,128]{1,0:T(8,128)(2,1)S(1)}, u32[]{:S(2)}, u32[]{:S(2)}) collective-permute-start(bf16[352,128]{1,0:T(8,128)(2,1)S(1)} %get-tuple-element.18), channel_id=1, source_target_pairs={{0,16},{8,24},{16,0},{24,8},{32,48},{40,56},{48,32},{56,40},{64,80... | collective-permute-start | bytes 270344 | tf_op jit(solution)/shard_map/ppermute | solution.py:37
  207.6 11.7 %collective-permute-start = (bf16[352,128]{1,0:T(8,128)(2,1)S(1)}, bf16[352,128]{1,0:T(8,128)(2,1)S(1)}, u32[]{:S(2)}, u32[]{:S(2)}) collective-permute-start(bf16[352,128]{1,0:T(8,128)(2,1)S(1)} %get-tuple-element.19), channel_id=1, source_target_pairs={{0,8},{8,0},{16,24},{24,16},{32,40},{40,32},{48,56},{56,48},{64,72... | collective-permute-start | bytes 270344 | tf_op jit(solution)/shard_map/ppermute | solution.py:37
  226.5 18.8 %all-to-all-start.8 = ((bf16[32,16,128]{2,1,0:T(8,128)(2,1)}), bf16[32,16,128]{2,1,0:T(8,128)(2,1)S(1)}, u32[]{:S(2)}, u32[]{:S(2)}) async-start(bf16[32,16,128]{2,1,0:T(8,128)(2,1)} %bitcast.30), calls=%async_computation.8 | async-start | bytes 262144 | tf_op jit(solution)/shard_map/all_to_all | solution.py:14

commit v2 on v1

--- a/solution.py
+++ b/solution.py
@@ -2,6 +2,7 @@
 import jax.numpy as jnp
 from jax import lax
 from jax.sharding import PartitionSpec as P
+
 
 D = 4096
 NEAR = 4
@@ -39,7 +40,7 @@
     return jnp.stack([pick(got, j ^ place) for j in range(NEAR)])
 
 
-def body(
+def step(
     tokens,
     mix_gain,
     w_query,
@@ -83,13 +84,14 @@
     block_f = block.astype(f32)
     normed = (block_f * mix_gain.astype(f32)[:, None]).astype(bf16)
     squares = jnp.sum(block_f * block_f, axis=0)
-    weights = (w_query, w_forget, w_input, w_outgate)
-    terms = [dot_t(normed, w, ((0,), (0,))).astype(bf16) for w in weights]
+    weights = jnp.concatenate([w_query, w_forget, w_input, w_outgate], axis=1)
+    terms = dot_t(normed, lax.optimization_barrier(weights), ((0,), (0,))).astype(bf16)
     side = jnp.broadcast_to(squares.astype(bf16)[:, None], (batch, 128))
-    terms = jnp.concatenate(terms + [side], axis=1)
+    terms = jnp.concatenate([terms, side], axis=1)
     terms = terms.reshape(far, NEAR, rows_here, -1).transpose(1, 0, 2, 3)
     terms = summed(spread(terms, "kv", near_groups)).astype(bf16)
-    sums = summed(spread(terms, "kv", far_groups))
+    sums = spread(terms, "kv", far_groups)
+    sums = summed(sums)
     key_width = heads_here * head_size
     inv_rms = lax.rsqrt(sums[:, 4 * key_width : 4 * key_width + 1] / D + eps)
     raw = [
@@ -134,7 +136,7 @@
 
 def solution(mesh):
     return jax.shard_map(
-        body,
+        step,
         mesh=mesh,
         in_specs=(
             P("grp", ("kv", "tp")),

time: 247 us -> 244 us (0.988)
  no operation moved by 1% of the time
where the time goes in v2:
time: 244 us; the launch traced here: 243 us
  starting transfers between devices  107 us (44%)
  waiting for transfers between devices  80.4 us (33%)
  blocking collectives  41.3 us (17%)
  local copies, waits for them, and re-layouts  6.84 us (3%)
  other arithmetic  5.55 us (2%)
    all_to_all x7, starting transfers between devices, spread(): lax.all_to_all(parts, axis, 0, 0, axis_index_groups=groups, tiled=True)  87.9 us
    all_to_all x7, waiting for transfers between devices, spread(): lax.all_to_all(parts, axis, 0, 0, axis_index_groups=groups, tiled=True)  63.8 us
    all_to_all x2, blocking collectives, spread(): lax.all_to_all(parts, axis, 0, 0, axis_index_groups=groups, tiled=True)  41.3 us
    ppermute x6, starting transfers between devices, exchanged(): got.append(lax.ppermute(pick(stack, place ^ k), 'kv', pairs))  18.7 us
    ppermute x6, waiting for transfers between devices, exchanged(): got.append(lax.ppermute(pick(stack, place ^ k), 'kv', pairs))  16.6 us
  transfers between devices with their start and end apart: 13, of which 8 were waited for; matrix products, arithmetic and copies ran while one was open for 1% of the time, Pallas kernels for 0%

profile of v2, /device:TPU:33, one launch (start us, length us, event | category | flops | bytes accessed | tf_op | source)
XLA Modules:
  0.0 243.4 jit_solution(17984628951318504831)
XLA Ops:
  0.7 1.4 broadcast_in_dim.21
  2.0 44.7 %all-to-all-start = ((bf16[8,16,128]{2,1,0:T(8,128)(2,1)}), bf16[8,16,128]{2,1,0:T(8,128)(2,1)S(1)}, u32[]{:S(2)}, u32[]{:S(2)}) async-start(bf16[8,16,128]{2,1,0:T(8,128)(2,1)} %broadcast_in_dim.21), calls=%async_computation | async-start | bytes 65536 | tf_op jit(solution)/shard_map/all_to_all | solution.py:15
  46.7 0.9 pad_maximum_fusion.9
  47.7 3.8 %all-to-all-done = bf16[8,16,128]{2,1,0:T(8,128)(2,1)S(1)} async-done(((bf16[8,16,128]{2,1,0:T(8,128)(2,1)}), bf16[8,16,128]{2,1,0:T(8,128)(2,1)S(1)}, u32[]{:S(2)}, u32[]{:S(2)}) %all-to-all-start) | async-done | bytes 32800 | tf_op jit(solution)/shard_map/all_to_all | solution.py:15
  51.5 0.1 fusion.23
  51.6 0.2 convolution_convert_fusion
  51.9 0.1 broadcast_in_dim.22
  52.0 0.1 reshape.122
  52.1 0.1 copy.123
  52.2 11.1 %all_to_all.45 = bf16[4,8,4,1152]{3,2,1,0:T(4,128)(2,1)S(1)} all-to-all(bf16[4,8,4,1152]{3,2,1,0:T(4,128)(2,1)S(1)} %bitcast.75), channel_id=1, replica_groups={{0,8,16,24},{32,40,48,56},{64,72,80,88},{96,104,112,120},{128,136,144,1..., dimensions={0} | all-to-all | bytes 589824 | tf_op jit(solution)/shard_map/all_to_all | solution.py:15
  63.3 0.8 reduce_sum.85
  64.1 6.7 %all-to-all-start.2 = ((bf16[8,4,1152]{2,1,0:T(4,128)(2,1)}), bf16[8,4,1152]{2,1,0:T(4,128)(2,1)S(1)}, u32[]{:S(2)}, u32[]{:S(2)}) async-start(bf16[8,4,1152]{2,1,0:T(4,128)(2,1)} %reduce_sum.85), calls=%async_computation.2 | async-start | bytes 147456 | tf_op jit(solution)/shard_map/all_to_all | solution.py:15
  70.8 0.7 copy-done.6
  71.5 23.3 %all-to-all-done.2 = bf16[8,4,1152]{2,1,0:T(4,128)(2,1)S(1)} async-done(((bf16[8,4,1152]{2,1,0:T(4,128)(2,1)}), bf16[8,4,1152]{2,1,0:T(4,128)(2,1)S(1)}, u32[]{:S(2)}, u32[]{:S(2)}) %all-to-all-start.2) | async-done | bytes 73760 | tf_op jit(solution)/shard_map/all_to_all | solution.py:15
  94.8 0.1 convert_reduce_fusion.3
  94.8 0.1 fusion.35
  94.9 0.1 add_divide_fusion.1
  95.1 1.3 multiply_reduce_fusion
  96.4 0.1 multiply_reduce_fusion.1
  96.5 0.1 multiply_bitcast_fusion
  96.6 0.1 fusion.32
  96.7 0.7 broadcast_in_dim.23
  97.3 4.8 %all-to-all-start.3 = ((bf16[32,4,256]{2,1,0:T(4,128)(2,1)}), bf16[32,4,256]{2,1,0:T(4,128)(2,1)S(1)}, u32[]{:S(2)}, u32[]{:S(2)}) async-start(bf16[32,4,256]{2,1,0:T(4,128)(2,1)} %broadcast_in_dim.23), calls=%async_computation.3 | async-start | bytes 131072 | tf_op jit(solution)/shard_map/all_to_all | solution.py:15
  102.1 0.6 copy-done.7
  102.8 0.1 copy.107
  102.9 0.1 pad.27.clone
  103.0 0.3 fusion.37
  103.3 0.3 fusion.13
  103.6 21.0 %all-to-all-done.3 = bf16[32,4,256]{2,1,0:T(4,128)(2,1)S(1)} async-done(((bf16[32,4,256]{2,1,0:T(4,128)(2,1)}), bf16[32,4,256]{2,1,0:T(4,128)(2,1)S(1)}, u32[]{:S(2)}, u32[]{:S(2)}) %all-to-all-start.3) | async-done | bytes 65568 | tf_op jit(solution)/shard_map/all_to_all | solution.py:15
  124.7 0.1 fusion.2
  124.9 0.1 copy.105
  125.0 0.7 broadcast_in_dim.24
  125.7 7.9 %all-to-all-start.4 = ((bf16[8,128,128]{2,1,0:T(8,128)(2,1)}), bf16[8,128,128]{2,1,0:T(8,128)(2,1)S(1)}, u32[]{:S(2)}, u32[]{:S(2)}) async-start(bf16[8,128,128]{2,1,0:T(8,128)(2,1)} %broadcast_in_dim.24), calls=%async_computation.4 | async-start | bytes 524288 | tf_op jit(solution)/shard_map/all_to_all | solution.py:15
  133.7 0.1 pad_maximum_fusion
  133.8 0.1 constant_dynamic-slice_fusion.4
  133.8 2.2 collective-permute-start.5
  136.0 3.1 %collective-permute-start.4 = (bf16[128,768]{1,0:T(8,128)(2,1)S(1)}, bf16[128,768]{1,0:T(8,128)(2,1)S(1)}, u32[]{:S(2)}, u32[]{:S(2)}) collective-permute-start(bf16[128,768]{1,0:T(8,128)(2,1)S(1)} %get-tuple-element.10), channel_id=1, source_target_pairs={{0,16},{8,24},{16,0},{24,8},{32,48},{40,56},{48,32},{56,40},{64,80... | collective-permute-start | bytes 589832 | tf_op jit(solution)/shard_map/ppermute | solution.py:38
  139.1 4.1 %collective-permute-start.3 = (bf16[128,768]{1,0:T(8,128)(2,1)S(1)}, bf16[128,768]{1,0:T(8,128)(2,1)S(1)}, u32[]{:S(2)}, u32[]{:S(2)}) collective-permute-start(bf16[128,768]{1,0:T(8,128)(2,1)S(1)} %get-tuple-element.11), channel_id=1, source_target_pairs={{0,8},{8,0},{16,24},{24,16},{32,40},{40,32},{48,56},{56,48},{64,72... | collective-permute-start | bytes 589832 | tf_op jit(solution)/shard_map/ppermute | solution.py:38
  143.3 0.1 copy.106
  143.4 0.7 broadcast_in_dim.25
  144.1 3.4 %all-to-all-start.5 = ((bf16[4,128,128]{1,2,0:T(8,128)(2,1)}), bf16[4,128,128]{1,2,0:T(8,128)(2,1)S(1)}, u32[]{:S(2)}, u32[]{:S(2)}) async-start(bf16[4,128,128]{1,2,0:T(8,128)(2,1)} %broadcast_in_dim.25), calls=%async_computation.5 | async-start | bytes 262144 | tf_op jit(solution)/shard_map/all_to_all | solution.py:15
  147.5 8.4 %collective-permute-done.4 = bf16[128,768]{1,0:T(8,128)(2,1)S(1)} collective-permute-done((bf16[128,768]{1,0:T(8,128)(2,1)S(1)}, bf16[128,768]{1,0:T(8,128)(2,1)S(1)}, u32[]{:S(2)}, u32[]{:S(2)}) %collective-permute-start.4) | collective-permute-done | bytes 196640 | tf_op jit(solution)/shard_map/ppermute | solution.py:38
  155.9 0.1 pad_maximum_fusion.1
  156.0 0.1 constant_dynamic-slice_fusion.3
  156.1 0.1 pad_maximum_fusion.2
  156.2 0.1 slice_convert_fusion
  156.3 0.1 copy.117
  156.4 0.9 all-to-all-done.5
  157.3 0.1 fusion.10
  157.5 0.3 fusion.1
  157.7 30.2 %all_to_all.46 = bf16[8,16,768]{2,1,0:T(8,128)(2,1)S(1)} all-to-all(bf16[8,16,768]{2,1,0:T(8,128)(2,1)S(1)} %bitcast.76), channel_id=1, replica_groups={{0,32,64,96,128,160,192,224},{8,40,72,104,136,168,200,232},{16,48,80,11..., dimensions={0} | all-to-all | bytes 393216 | tf_op jit(solution)/shard_map/all_to_all | solution.py:15
  188.0 0.2 fusion.29
  188.2 0.1 fusion.26
  188.3 0.6 broadcast_in_dim.29
  188.9 10.2 %all-to-all-start.7 = ((bf16[8,16,352]{2,1,0:T(8,128)(2,1)}), bf16[8,16,352]{2,1,0:T(8,128)(2,1)S(1)}, u32[]{:S(2)}, u32[]{:S(2)}) async-start(bf16[8,16,352]{2,1,0:T(8,128)(2,1)} %broadcast_in_dim.29), calls=%async_computation.7 | async-start | bytes 196608 | tf_op jit(solution)/shard_map/all_to_all | solution.py:15
  199.2 3.9 %collective-permute-start.2 = (bf16[352,128]{1,0:T(8,128)(2,1)S(1)}, bf16[352,128]{1,0:T(8,128)(2,1)S(1)}, u32[]{:S(2)}, u32[]{:S(2)}) collective-permute-start(bf16[352,128]{1,0:T(8,128)(2,1)S(1)} %get-tuple-element.17), channel_id=1, source_target_pairs={{0,24},{8,16},{16,8},{24,0},{32,56},{40,48},{48,40},{56,32},{64,88... | collective-permute-start | bytes 270344 | tf_op jit(solution)/shard_map/ppermute | solution.py:38
  203.1 2.0 collective-permute-start.1
  205.1 3.5 %collective-permute-start = (bf16[352,128]{1,0:T(8,128)(2,1)S(1)}, bf16[352,128]{1,0:T(8,128)(2,1)S(1)}, u32[]{:S(2)}, u32[]{:S(2)}) collective-permute-start(bf16[352,128]{1,0:T(8,128)(2,1)S(1)} %get-tuple-element.19), channel_id=1, source_target_pairs={{0,8},{8,0},{16,24},{24,16},{32,40},{40,32},{48,56},{56,48},{64,72... | collective-permute-start | bytes 270344 | tf_op jit(solution)/shard_map/ppermute | solution.py:38
  208.6 8.2 %collective-permute-done.1 = bf16[352,128]{1,0:T(8,128)(2,1)S(1)} collective-permute-done((bf16[352,128]{1,0:T(8,128)(2,1)S(1)}, bf16[352,128]{1,0:T(8,128)(2,1)S(1)}, u32[]{:S(2)}, u32[]{:S(2)}) %collective-permute-start.1) | collective-permute-done | bytes 90144 | tf_op jit(solution)/shard_map/ppermute | solution.py:38
  216.9 6.3 %all-to-all-done.7 = bf16[8,16,352]{2,1,0:T(8,128)(2,1)S(1)} async-done(((bf16[8,16,352]{2,1,0:T(8,128)(2,1)}), bf16[8,16,352]{2,1,0:T(8,128)(2,1)S(1)}, u32[]{:S(2)}, u32[]{:S(2)}) %all-to-all-start.7) | async-done | bytes 90144 | tf_op jit(solution)/shard_map/all_to_all | solution.py:15
  223.2 0.9 convolution_convert_fusion.1
  224.1 10.2 %all-to-all-start.8 = ((bf16[32,16,128]{2,1,0:T(8,128)(2,1)}), bf16[32,16,128]{2,1,0:T(8,128)(2,1)S(1)}, u32[]{:S(2)}, u32[]{:S(2)}) async-start(bf16[32,16,128]{2,1,0:T(8,128)(2,1)} %bitcast.30), calls=%async_computation.8 | async-start | bytes 262144 | tf_op jit(solution)/shard_map/all_to_all | solution.py:15
  234.3 8.4 %all-to-all-done.8 = bf16[32,16,128]{2,1,0:T(8,128)(2,1)S(1)} async-done(((bf16[32,16,128]{2,1,0:T(8,128)(2,1)}), bf16[32,16,128]{2,1,0:T(8,128)(2,1)S(1)}, u32[]{:S(2)}, u32[]{:S(2)}) %all-to-all-start.8) | async-done | bytes 131104 | tf_op jit(solution)/shard_map/all_to_all | solution.py:15
  242.8 0.6 fusion.31
  (45 shorter events, 0.5 us)
Async XLA Ops:
  0.6 124.1 %copy-start = (bf16[256,128]{1,0:T(8,128)(2,1)S(1)}, bf16[256,128]{1,0:T(8,128)(2,1)}, u32[]{:S(2)}) copy-start(bf16[256,128]{1,0:T(8,128)(2,1)} %param.23) | copy-start | bytes 196612
  0.6 46.1 %copy-start.5 = (bf16[128,256]{1,0:T(8,128)(2,1)S(1)}, bf16[128,256]{1,0:T(8,128)(2,1)}, u32[]{:S(2)}) copy-start(bf16[128,256]{1,0:T(8,128)(2,1)} %param.19) | copy-start | bytes 196612
  2.0 49.5 %all-to-all-start = ((bf16[8,16,128]{2,1,0:T(8,128)(2,1)}), bf16[8,16,128]{2,1,0:T(8,128)(2,1)S(1)}, u32[]{:S(2)}, u32[]{:S(2)}) async-start(bf16[8,16,128]{2,1,0:T(8,128)(2,1)} %broadcast_in_dim.21), calls=%async_computation | async-start | bytes 65536 | tf_op jit(solution)/shard_map/all_to_all | solution.py:15
  46.7 0.9 copy-start.8
  52.2 42.9 %copy-start.1 = (f32[4,2,128,128]{3,2,1,0:T(8,128)S(1)}, f32[4,2,128,128]{3,2,1,0:T(8,128)}, u32[]{:S(2)}) copy-start(f32[4,2,128,128]{3,2,1,0:T(8,128)} %param.21) | copy-start | bytes 1572868
  64.1 6.7 %copy-start.9 = (bf16[128]{0:T(256)(128)(2,1)S(1)}, bf16[128]{0:T(256)(128)(2,1)}, u32[]{:S(2)}) copy-start(bf16[128]{0:T(256)(128)(2,1)} %param.22) | copy-start | bytes 772
  64.1 30.7 %all-to-all-start.2 = ((bf16[8,4,1152]{2,1,0:T(4,128)(2,1)}), bf16[8,4,1152]{2,1,0:T(4,128)(2,1)S(1)}, u32[]{:S(2)}, u32[]{:S(2)}) async-start(bf16[8,4,1152]{2,1,0:T(4,128)(2,1)} %reduce_sum.85), calls=%async_computation.2 | async-start | bytes 147456 | tf_op jit(solution)/shard_map/all_to_all | solution.py:15
  70.8 0.7 copy-start.6
  95.1 7.9 %copy-start.2 = (bf16[128,1408]{1,0:T(8,128)(2,1)S(1)}, bf16[128,1408]{1,0:T(8,128)(2,1)}, u32[]{:S(2)}) copy-start(bf16[128,1408]{1,0:T(8,128)(2,1)} %param.25) | copy-start | bytes 1081348
  95.1 7.9 %copy-start.3 = (bf16[128,1408]{1,0:T(8,128)(2,1)S(1)}, bf16[128,1408]{1,0:T(8,128)(2,1)}, u32[]{:S(2)}) copy-start(bf16[128,1408]{1,0:T(8,128)(2,1)} %param.26) | copy-start | bytes 1081348
  97.3 27.4 %all-to-all-start.3 = ((bf16[32,4,256]{2,1,0:T(4,128)(2,1)}), bf16[32,4,256]{2,1,0:T(4,128)(2,1)S(1)}, u32[]{:S(2)}, u32[]{:S(2)}) async-start(bf16[32,4,256]{2,1,0:T(4,128)(2,1)} %broadcast_in_dim.23), calls=%async_computation.3 | async-start | bytes 131072 | tf_op jit(solution)/shard_map/all_to_all | solution.py:15
  102.1 0.7 copy-start.7
  125.7 17.5 %all-to-all-start.4 = ((bf16[8,128,128]{2,1,0:T(8,128)(2,1)}), bf16[8,128,128]{2,1,0:T(8,128)(2,1)S(1)}, u32[]{:S(2)}, u32[]{:S(2)}) async-start(bf16[8,128,128]{2,1,0:T(8,128)(2,1)} %broadcast_in_dim.24), calls=%async_computation.4 | async-start | bytes 524288 | tf_op jit(solution)/shard_map/all_to_all | solution.py:15
  133.8 13.7 %collective-permute-start.5 = (bf16[128,768]{1,0:T(8,128)(2,1)S(1)}, bf16[128,768]{1,0:T(8,128)(2,1)S(1)}, u32[]{:S(2)}, u32[]{:S(2)}) collective-permute-start(bf16[128,768]{1,0:T(8,128)(2,1)S(1)} %get-tuple-element.9), channel_id=1, source_target_pairs={{0,24},{8,16},{16,8},{24,0},{32,56},{40,48},{48,40},{56,32},{64,88... | collective-permute-start | bytes 589832 | tf_op jit(solution)/shard_map/ppermute | solution.py:38
  136.0 19.9 %collective-permute-start.4 = (bf16[128,768]{1,0:T(8,128)(2,1)S(1)}, bf16[128,768]{1,0:T(8,128)(2,1)S(1)}, u32[]{:S(2)}, u32[]{:S(2)}) collective-permute-start(bf16[128,768]{1,0:T(8,128)(2,1)S(1)} %get-tuple-element.10), channel_id=1, source_target_pairs={{0,16},{8,24},{16,0},{24,8},{32,48},{40,56},{48,32},{56,40},{64,80... | collective-permute-start | bytes 589832 | tf_op jit(solution)/shard_map/ppermute | solution.py:38
  139.1 16.8 %collective-permute-start.3 = (bf16[128,768]{1,0:T(8,128)(2,1)S(1)}, bf16[128,768]{1,0:T(8,128)(2,1)S(1)}, u32[]{:S(2)}, u32[]{:S(2)}) collective-permute-start(bf16[128,768]{1,0:T(8,128)(2,1)S(1)} %get-tuple-element.11), channel_id=1, source_target_pairs={{0,8},{8,0},{16,24},{24,16},{32,40},{40,32},{48,56},{56,48},{64,72... | collective-permute-start | bytes 589832 | tf_op jit(solution)/shard_map/ppermute | solution.py:38
  144.1 13.3 %all-to-all-start.5 = ((bf16[4,128,128]{1,2,0:T(8,128)(2,1)}), bf16[4,128,128]{1,2,0:T(8,128)(2,1)S(1)}, u32[]{:S(2)}, u32[]{:S(2)}) async-start(bf16[4,128,128]{1,2,0:T(8,128)(2,1)} %broadcast_in_dim.25), calls=%async_computation.5 | async-start | bytes 262144 | tf_op jit(solution)/shard_map/all_to_all | solution.py:15
  187.9 11.2 %copy-start.4 = (bf16[1408,128]{1,0:T(8,128)(2,1)S(1)}, bf16[1408,128]{1,0:T(8,128)(2,1)}, u32[]{:S(2)}) copy-start(bf16[1408,128]{1,0:T(8,128)(2,1)} %param.27) | copy-start | bytes 1081348
  188.9 34.3 %all-to-all-start.7 = ((bf16[8,16,352]{2,1,0:T(8,128)(2,1)}), bf16[8,16,352]{2,1,0:T(8,128)(2,1)S(1)}, u32[]{:S(2)}, u32[]{:S(2)}) async-start(bf16[8,16,352]{2,1,0:T(8,128)(2,1)} %broadcast_in_dim.29), calls=%async_computation.7 | async-start | bytes 196608 | tf_op jit(solution)/shard_map/all_to_all | solution.py:15
  199.2 9.4 %collective-permute-start.2 = (bf16[352,128]{1,0:T(8,128)(2,1)S(1)}, bf16[352,128]{1,0:T(8,128)(2,1)S(1)}, u32[]{:S(2)}, u32[]{:S(2)}) collective-permute-start(bf16[352,128]{1,0:T(8,128)(2,1)S(1)} %get-tuple-element.17), channel_id=1, source_target_pairs={{0,24},{8,16},{16,8},{24,0},{32,56},{40,48},{48,40},{56,32},{64,88... | collective-permute-start | bytes 270344 | tf_op jit(solution)/shard_map/ppermute | solution.py:38
  203.1 13.6 %collective-permute-start.1 = (bf16[352,128]{1,0:T(8,128)(2,1)S(1)}, bf16[352,128]{1,0:T(8,128)(2,1)S(1)}, u32[]{:S(2)}, u32[]{:S(2)}) collective-permute-start(bf16[352,128]{1,0:T(8,128)(2,1)S(1)} %get-tuple-element.18), channel_id=1, source_target_pairs={{0,16},{8,24},{16,0},{24,8},{32,48},{40,56},{48,32},{56,40},{64,80... | collective-permute-start | bytes 270344 | tf_op jit(solution)/shard_map/ppermute | solution.py:38
  205.1 11.7 %collective-permute-start = (bf16[352,128]{1,0:T(8,128)(2,1)S(1)}, bf16[352,128]{1,0:T(8,128)(2,1)S(1)}, u32[]{:S(2)}, u32[]{:S(2)}) collective-permute-start(bf16[352,128]{1,0:T(8,128)(2,1)S(1)} %get-tuple-element.19), channel_id=1, source_target_pairs={{0,8},{8,0},{16,24},{24,16},{32,40},{40,32},{48,56},{56,48},{64,72... | collective-permute-start | bytes 270344 | tf_op jit(solution)/shard_map/ppermute | solution.py:38
  224.1 18.7 %all-to-all-start.8 = ((bf16[32,16,128]{2,1,0:T(8,128)(2,1)}), bf16[32,16,128]{2,1,0:T(8,128)(2,1)S(1)}, u32[]{:S(2)}, u32[]{:S(2)}) async-start(bf16[32,16,128]{2,1,0:T(8,128)(2,1)} %bitcast.30), calls=%async_computation.8 | async-start | bytes 262144 | tf_op jit(solution)/shard_map/all_to_all | solution.py:15

commit v3 on v2

--- a/solution.py
+++ b/solution.py
@@ -71,14 +71,18 @@
     width = -(-(2 * units + 1) // 128) * 128
     pad = jnp.zeros((w_gate.shape[0], width - 2 * units - 1), bf16)
     cut = lambda w, j: w[:, j * units : (j + 1) * units]
-    pieces = jnp.stack(
-        [
-            jnp.concatenate([cut(w_gate, j), cut(w_up, j), ffn_gain[:, None], pad], axis=1)
-            for j in range(NEAR)
-        ]
+    rows = w_gate.shape[0]
+    pieces = []
+    for j in range(NEAR):
+        both = jnp.concatenate([cut(w_gate, j), cut(w_up, j), ffn_gain[:, None], pad], axis=1)
+        blocks = [both[:, at : at + 128] for at in range(0, width, 128)]
+        pieces.append(jnp.concatenate(blocks + [w_down[j * units : (j + 1) * units]], axis=0))
+    got = exchanged(jnp.stack(pieces), place, near_groups)
+    at_down = width // 128 * rows
+    w_out = got[:, at_down:]
+    w_gate_up = jnp.concatenate(
+        [got[:, at : at + rows].reshape(-1, 128) for at in range(0, at_down, rows)], axis=1
     )
-    w_gate_up = exchanged(pieces, place, near_groups).reshape(-1, width)
-    w_out = exchanged(w_down.reshape(NEAR, units, -1), place, near_groups)
 
     block = share(tokens.T, "tp", tp).reshape(-1, batch)
     block_f = block.astype(f32)

time: 244 us -> 253 us (1.037)
  blocking collectives: 41.3 us -> 31.5 us
  waiting for transfers between devices: 80.4 us -> 87.7 us
  starting transfers between devices: 107 us -> 114 us
  local copies, waits for them, and re-layouts: 6.84 us -> 9.73 us
    all_to_all x7 -> x8, waiting for transfers between devices: 63.8 us -> 87.7 us  [spread(): lax.all_to_all(parts, axis, 0, 0, axis_index_groups=groups, tiled=True)]
    ppermute x6 -> x3, waiting for transfers between devices: 16.6 us -> 0.01 us  [exchanged(): got.append(lax.ppermute(pick(stack, place ^ k), 'kv', pairs))]
    all_to_all x7 -> x8, starting transfers between devices: 87.9 us -> 104 us  [spread(): lax.all_to_all(parts, axis, 0, 0, axis_index_groups=groups, tiled=True)]
    all_to_all x2 -> x1, blocking collectives: 41.3 us -> 31.5 us  [spread(): lax.all_to_all(parts, axis, 0, 0, axis_index_groups=groups, tiled=True)]
    ppermute x6 -> x3, starting transfers between devices: 18.7 us -> 9.5 us  [exchanged(): got.append(lax.ppermute(pick(stack, place ^ k), 'kv', pairs))]
  transfers between devices with their start and end apart: 13 -> 11, of which waited for: 8 -> 6; matrix products, arithmetic and copies ran while one was open for 1% -> 4% of each run, Pallas kernels for 0% -> 0%
where the time goes in v3:
time: 253 us; the launch traced here: 252 us
  starting transfers between devices  114 us (45%)
  waiting for transfers between devices  87.7 us (35%)
  blocking collectives  31.5 us (12%)
  local copies, waits for them, and re-layouts  9.73 us (4%)
  other arithmetic  5.84 us (2%)
    all_to_all x8, starting transfers between devices, spread(): lax.all_to_all(parts, axis, 0, 0, axis_index_groups=groups, tiled=True)  104 us
    all_to_all x8, waiting for transfers between devices, spread(): lax.all_to_all(parts, axis, 0, 0, axis_index_groups=groups, tiled=True)  87.7 us
    all_to_all x1, blocking collectives, spread(): lax.all_to_all(parts, axis, 0, 0, axis_index_groups=groups, tiled=True)  31.5 us
    ppermute x3, starting transfers between devices, exchanged(): got.append(lax.ppermute(pick(stack, place ^ k), 'kv', pairs))  9.5 us
  transfers between devices with their start and end apart: 11, of which 6 were waited for; matrix products, arithmetic and copies ran while one was open for 4% of the time, Pallas kernels for 0%

profile of v3, /device:TPU:33, one launch (start us, length us, event | category | flops | bytes accessed | tf_op | source)
XLA Modules:
  0.0 251.5 jit_solution(10837036288783469185)
XLA Ops:
  0.7 1.4 broadcast_in_dim.21
  2.0 44.7 %all-to-all-start = ((bf16[8,16,128]{2,1,0:T(8,128)(2,1)}), bf16[8,16,128]{2,1,0:T(8,128)(2,1)S(1)}, u32[]{:S(2)}, u32[]{:S(2)}) async-start(bf16[8,16,128]{2,1,0:T(8,128)(2,1)} %broadcast_in_dim.21), calls=%async_computation | async-start | bytes 65536 | tf_op jit(solution)/shard_map/all_to_all | solution.py:15
  46.7 1.0 constant_dynamic-update-slice_fusion.5
  47.8 1.2 fusion.22
  49.0 0.2 fusion.23
  49.2 1.0 constant_dynamic-update-slice_fusion.4
  50.2 0.9 constant_dynamic-update-slice_fusion.15
  51.3 0.1 copy.99
  51.5 0.1 fusion.5
  51.6 0.2 convolution_convert_fusion
  51.9 0.1 broadcast_in_dim.22
  52.0 0.1 reshape.129
  52.1 0.8 copy.115
  52.9 3.7 %all-to-all-start.1 = ((bf16[4,8,4,1152]{3,2,1,0:T(4,128)(2,1)}), bf16[4,8,4,1152]{3,2,1,0:T(4,128)(2,1)S(1)}, u32[]{:S(2)}, u32[]{:S(2)}) async-start(bf16[4,8,4,1152]{3,2,1,0:T(4,128)(2,1)} %bitcast.63), calls=%async_computation.1 | async-start | bytes 589824 | tf_op jit(solution)/shard_map/all_to_all | solution.py:15
  56.6 0.1 pad_slice_fusion
  56.6 0.1 constant_dynamic-update-slice_fusion.21
  56.7 0.1 constant_dynamic-update-slice_fusion.3
  56.8 0.1 constant_dynamic-update-slice_fusion.2
  57.0 0.1 constant_dynamic-update-slice_fusion.1
  57.1 0.1 constant_dynamic-update-slice_fusion
  57.3 0.1 pad_maximum_fusion
  57.5 0.1 constant_dynamic-slice_fusion.4
  57.6 3.4 %collective-permute-start = (bf16[1120,128]{1,0:T(8,128)(2,1)S(1)}, bf16[1120,128]{1,0:T(8,128)(2,1)S(1)}, u32[]{:S(2)}, u32[]{:S(2)}) collective-permute-start(bf16[1120,128]{1,0:T(8,128)(2,1)S(1)} %get-tuple-element.17), channel_id=1, source_target_pairs={{0,8},{8,0},{16,24},{24,16},{32,40},{40,32},{48,56},{56,48},{64,72... | collective-permute-start | bytes 860168 | tf_op jit(solution)/shard_map/ppermute | solution.py:38
  61.0 4.1 %collective-permute-start.1 = (bf16[1120,128]{1,0:T(8,128)(2,1)S(1)}, bf16[1120,128]{1,0:T(8,128)(2,1)S(1)}, u32[]{:S(2)}, u32[]{:S(2)}) collective-permute-start(bf16[1120,128]{1,0:T(8,128)(2,1)S(1)} %get-tuple-element.16), channel_id=1, source_target_pairs={{0,16},{8,24},{16,0},{24,8},{32,48},{40,56},{48,32},{56,40},{64,80... | collective-permute-start | bytes 860168 | tf_op jit(solution)/shard_map/ppermute | solution.py:38
  65.1 2.0 collective-permute-start.2
  67.1 0.8 reduce_sum.85
  67.9 6.4 %all-to-all-start.2 = ((bf16[8,4,1152]{2,1,0:T(4,128)(2,1)}), bf16[8,4,1152]{2,1,0:T(4,128)(2,1)S(1)}, u32[]{:S(2)}, u32[]{:S(2)}) async-start(bf16[8,4,1152]{2,1,0:T(4,128)(2,1)} %reduce_sum.85), calls=%async_computation.2 | async-start | bytes 147456 | tf_op jit(solution)/shard_map/all_to_all | solution.py:15
  74.4 23.0 %all-to-all-done.2 = bf16[8,4,1152]{2,1,0:T(4,128)(2,1)S(1)} async-done(((bf16[8,4,1152]{2,1,0:T(4,128)(2,1)}), bf16[8,4,1152]{2,1,0:T(4,128)(2,1)S(1)}, u32[]{:S(2)}, u32[]{:S(2)}) %all-to-all-start.2) | async-done | bytes 73760 | tf_op jit(solution)/shard_map/all_to_all | solution.py:15
  97.4 0.1 convert_reduce_fusion.3
  97.4 0.1 fusion.21
  97.5 0.1 add_divide_fusion.1
  97.7 1.3 multiply_reduce_fusion
  99.0 0.1 multiply_reduce_fusion.2
  99.1 0.1 multiply_bitcast_fusion
  99.2 0.1 fusion.18
  99.3 0.6 broadcast_in_dim.23
  99.9 18.7 %all-to-all-start.3 = ((bf16[32,4,256]{2,1,0:T(4,128)(2,1)}), bf16[32,4,256]{2,1,0:T(4,128)(2,1)S(1)}, u32[]{:S(2)}, u32[]{:S(2)}) async-start(bf16[32,4,256]{2,1,0:T(4,128)(2,1)} %broadcast_in_dim.23), calls=%async_computation.3 | async-start | bytes 131072 | tf_op jit(solution)/shard_map/all_to_all | solution.py:15
  118.7 0.1 pad_maximum_fusion.1
  118.8 0.1 constant_dynamic-slice_fusion.3
  119.0 22.4 %all-to-all-done.3 = bf16[32,4,256]{2,1,0:T(4,128)(2,1)S(1)} async-done(((bf16[32,4,256]{2,1,0:T(4,128)(2,1)}), bf16[32,4,256]{2,1,0:T(4,128)(2,1)S(1)}, u32[]{:S(2)}, u32[]{:S(2)}) %all-to-all-start.3) | async-done | bytes 65568 | tf_op jit(solution)/shard_map/all_to_all | solution.py:15
  141.4 0.1 fusion.1
  141.5 0.1 copy.98
  141.7 0.7 broadcast_in_dim.24
  142.4 8.0 %all-to-all-start.4 = ((bf16[8,128,128]{2,1,0:T(8,128)(2,1)}), bf16[8,128,128]{2,1,0:T(8,128)(2,1)S(1)}, u32[]{:S(2)}, u32[]{:S(2)}) async-start(bf16[8,128,128]{2,1,0:T(8,128)(2,1)} %broadcast_in_dim.24), calls=%async_computation.4 | async-start | bytes 524288 | tf_op jit(solution)/shard_map/all_to_all | solution.py:15
  150.4 0.1 slice_convert_fusion
  150.5 0.1 copy.109
  150.6 6.3 %all-to-all-done.4 = bf16[8,128,128]{2,1,0:T(8,128)(2,1)S(1)} async-done(((bf16[8,128,128]{2,1,0:T(8,128)(2,1)}), bf16[8,128,128]{2,1,0:T(8,128)(2,1)S(1)}, u32[]{:S(2)}, u32[]{:S(2)}) %all-to-all-start.4) | async-done | bytes 262176 | tf_op jit(solution)/shard_map/all_to_all | solution.py:15
  156.9 0.7 broadcast_in_dim.27
  157.6 3.4 %all-to-all-start.5 = ((bf16[4,128,128]{2,1,0:T(8,128)(2,1)}), bf16[4,128,128]{2,1,0:T(8,128)(2,1)S(1)}, u32[]{:S(2)}, u32[]{:S(2)}) async-start(bf16[4,128,128]{2,1,0:T(8,128)(2,1)} %broadcast_in_dim.27), calls=%async_computation.5 | async-start | bytes 262144 | tf_op jit(solution)/shard_map/all_to_all | solution.py:15
  161.3 4.4 %all-to-all-done.5 = bf16[4,128,128]{2,1,0:T(8,128)(2,1)S(1)} async-done(((bf16[4,128,128]{2,1,0:T(8,128)(2,1)}), bf16[4,128,128]{2,1,0:T(8,128)(2,1)S(1)}, u32[]{:S(2)}, u32[]{:S(2)}) %all-to-all-start.5) | async-done | bytes 131104 | tf_op jit(solution)/shard_map/all_to_all | solution.py:15
  165.7 0.1 multiply_reduce_fusion.1
  165.8 0.1 fusion.3
  166.0 0.3 fusion
  166.3 31.5 %all_to_all.45 = bf16[8,16,768]{2,1,0:T(8,128)(2,1)S(1)} all-to-all(bf16[8,16,768]{2,1,0:T(8,128)(2,1)S(1)} %bitcast.66), channel_id=1, replica_groups={{0,32,64,96,128,160,192,224},{8,40,72,104,136,168,200,232},{16,48,80,11..., dimensions={0} | all-to-all | bytes 393216 | tf_op jit(solution)/shard_map/all_to_all | solution.py:15
  197.8 0.2 fusion.15
  198.0 0.1 fusion.12
  198.1 0.7 broadcast_in_dim.29
  198.7 9.8 %all-to-all-start.7 = ((bf16[8,16,352]{2,1,0:T(8,128)(2,1)}), bf16[8,16,352]{2,1,0:T(8,128)(2,1)S(1)}, u32[]{:S(2)}, u32[]{:S(2)}) async-start(bf16[8,16,352]{2,1,0:T(8,128)(2,1)} %broadcast_in_dim.29), calls=%async_computation.7 | async-start | bytes 196608 | tf_op jit(solution)/shard_map/all_to_all | solution.py:15
  208.5 0.1 pad_maximum_fusion.2
  208.6 23.1 %all-to-all-done.7 = bf16[8,16,352]{2,1,0:T(8,128)(2,1)S(1)} async-done(((bf16[8,16,352]{2,1,0:T(8,128)(2,1)}), bf16[8,16,352]{2,1,0:T(8,128)(2,1)S(1)}, u32[]{:S(2)}, u32[]{:S(2)}) %all-to-all-start.7) | async-done | bytes 90144 | tf_op jit(solution)/shard_map/all_to_all | solution.py:15
  231.8 1.0 convolution_convert_fusion.1
  232.7 9.7 %all-to-all-start.8 = ((bf16[32,16,128]{2,1,0:T(8,128)(2,1)}), bf16[32,16,128]{2,1,0:T(8,128)(2,1)S(1)}, u32[]{:S(2)}, u32[]{:S(2)}) async-start(bf16[32,16,128]{2,1,0:T(8,128)(2,1)} %bitcast.28), calls=%async_computation.8 | async-start | bytes 262144 | tf_op jit(solution)/shard_map/all_to_all | solution.py:15
  242.5 8.4 %all-to-all-done.8 = bf16[32,16,128]{2,1,0:T(8,128)(2,1)S(1)} async-done(((bf16[32,16,128]{2,1,0:T(8,128)(2,1)}), bf16[32,16,128]{2,1,0:T(8,128)(2,1)S(1)}, u32[]{:S(2)}, u32[]{:S(2)}) %all-to-all-start.8) | async-done | bytes 131104 | tf_op jit(solution)/shard_map/all_to_all | solution.py:15
  250.9 0.6 fusion.17
  (58 shorter events, 0.7 us)
Async XLA Ops:
  0.6 140.8 %copy-start = (bf16[256,128]{1,0:T(8,128)(2,1)S(1)}, bf16[256,128]{1,0:T(8,128)(2,1)}, u32[]{:S(2)}) copy-start(bf16[256,128]{1,0:T(8,128)(2,1)} %param.23) | copy-start | bytes 196612
  0.6 48.3 %copy-start.1 = (bf16[128,1408]{1,0:T(8,128)(2,1)S(1)}, bf16[128,1408]{1,0:T(8,128)(2,1)}, u32[]{:S(2)}) copy-start(bf16[128,1408]{1,0:T(8,128)(2,1)} %param.26) | copy-start | bytes 1081348
  2.0 49.5 %all-to-all-start = ((bf16[8,16,128]{2,1,0:T(8,128)(2,1)}), bf16[8,16,128]{2,1,0:T(8,128)(2,1)S(1)}, u32[]{:S(2)}, u32[]{:S(2)}) async-start(bf16[8,16,128]{2,1,0:T(8,128)(2,1)} %broadcast_in_dim.21), calls=%async_computation | async-start | bytes 65536 | tf_op jit(solution)/shard_map/all_to_all | solution.py:15
  46.7 4.5 %copy-start.4 = (bf16[128,256]{1,0:T(8,128)(2,1)S(1)}, bf16[128,256]{1,0:T(8,128)(2,1)}, u32[]{:S(2)}) copy-start(bf16[128,256]{1,0:T(8,128)(2,1)} %param.19) | copy-start | bytes 196612
  46.7 4.5 %copy-start.5 = (bf16[128,256]{1,0:T(8,128)(2,1)S(1)}, bf16[128,256]{1,0:T(8,128)(2,1)}, u32[]{:S(2)}) copy-start(bf16[128,256]{1,0:T(8,128)(2,1)} %param.18) | copy-start | bytes 196612
  46.7 4.5 %copy-start.6 = (bf16[128,256]{1,0:T(8,128)(2,1)S(1)}, bf16[128,256]{1,0:T(8,128)(2,1)}, u32[]{:S(2)}) copy-start(bf16[128,256]{1,0:T(8,128)(2,1)} %param.17) | copy-start | bytes 196612
  46.7 4.5 %copy-start.7 = (bf16[128,256]{1,0:T(8,128)(2,1)S(1)}, bf16[128,256]{1,0:T(8,128)(2,1)}, u32[]{:S(2)}) copy-start(bf16[128,256]{1,0:T(8,128)(2,1)} %param.16) | copy-start | bytes 196612
  49.0 2.3 copy-start.9
  49.0 2.4 copy-start.10
  52.9 4.4 %copy-start.3 = (bf16[1408,128]{1,0:T(8,128)(2,1)S(1)}, bf16[1408,128]{1,0:T(8,128)(2,1)}, u32[]{:S(2)}) copy-start(bf16[1408,128]{1,0:T(8,128)(2,1)} %param.27) | copy-start | bytes 1081348
  52.9 14.3 %all-to-all-start.1 = ((bf16[4,8,4,1152]{3,2,1,0:T(4,128)(2,1)}), bf16[4,8,4,1152]{3,2,1,0:T(4,128)(2,1)S(1)}, u32[]{:S(2)}, u32[]{:S(2)}) async-start(bf16[4,8,4,1152]{3,2,1,0:T(4,128)(2,1)} %bitcast.63), calls=%async_computation.1 | async-start | bytes 589824 | tf_op jit(solution)/shard_map/all_to_all | solution.py:15
  57.5 9.7 %copy-start.11 = (bf16[128]{0:T(256)(128)(2,1)S(1)}, bf16[128]{0:T(256)(128)(2,1)}, u32[]{:S(2)}) copy-start(bf16[128]{0:T(256)(128)(2,1)} %param.22) | copy-start | bytes 772
  57.5 16.9 %copy-start.8 = (f32[256]{0:T(256)S(1)}, f32[256]{0:T(256)}, u32[]{:S(2)}) copy-start(f32[256]{0:T(256)} %param.20) | copy-start | bytes 3076
  57.5 40.2 %copy-start.2 = (f32[4,2,128,128]{3,2,1,0:T(8,128)S(1)}, f32[4,2,128,128]{3,2,1,0:T(8,128)}, u32[]{:S(2)}) copy-start(f32[4,2,128,128]{3,2,1,0:T(8,128)} %param.21) | copy-start | bytes 1572868
  57.6 61.1 %collective-permute-start = (bf16[1120,128]{1,0:T(8,128)(2,1)S(1)}, bf16[1120,128]{1,0:T(8,128)(2,1)S(1)}, u32[]{:S(2)}, u32[]{:S(2)}) collective-permute-start(bf16[1120,128]{1,0:T(8,128)(2,1)S(1)} %get-tuple-element.17), channel_id=1, source_target_pairs={{0,8},{8,0},{16,24},{24,16},{32,40},{40,32},{48,56},{56,48},{64,72... | collective-permute-start | bytes 860168 | tf_op jit(solution)/shard_map/ppermute | solution.py:38
  61.0 57.7 %collective-permute-start.1 = (bf16[1120,128]{1,0:T(8,128)(2,1)S(1)}, bf16[1120,128]{1,0:T(8,128)(2,1)S(1)}, u32[]{:S(2)}, u32[]{:S(2)}) collective-permute-start(bf16[1120,128]{1,0:T(8,128)(2,1)S(1)} %get-tuple-element.16), channel_id=1, source_target_pairs={{0,16},{8,24},{16,0},{24,8},{32,48},{40,56},{48,32},{56,40},{64,80... | collective-permute-start | bytes 860168 | tf_op jit(solution)/shard_map/ppermute | solution.py:38
  65.1 53.6 %collective-permute-start.2 = (bf16[1120,128]{1,0:T(8,128)(2,1)S(1)}, bf16[1120,128]{1,0:T(8,128)(2,1)S(1)}, u32[]{:S(2)}, u32[]{:S(2)}) collective-permute-start(bf16[1120,128]{1,0:T(8,128)(2,1)S(1)} %get-tuple-element.15), channel_id=1, source_target_pairs={{0,24},{8,16},{16,8},{24,0},{32,56},{40,48},{48,40},{56,32},{64,88... | collective-permute-start | bytes 860168 | tf_op jit(solution)/shard_map/ppermute | solution.py:38
  67.9 29.5 %all-to-all-start.2 = ((bf16[8,4,1152]{2,1,0:T(4,128)(2,1)}), bf16[8,4,1152]{2,1,0:T(4,128)(2,1)S(1)}, u32[]{:S(2)}, u32[]{:S(2)}) async-start(bf16[8,4,1152]{2,1,0:T(4,128)(2,1)} %reduce_sum.85), calls=%async_computation.2 | async-start | bytes 147456 | tf_op jit(solution)/shard_map/all_to_all | solution.py:15
  99.9 41.5 %all-to-all-start.3 = ((bf16[32,4,256]{2,1,0:T(4,128)(2,1)}), bf16[32,4,256]{2,1,0:T(4,128)(2,1)S(1)}, u32[]{:S(2)}, u32[]{:S(2)}) async-start(bf16[32,4,256]{2,1,0:T(4,128)(2,1)} %broadcast_in_dim.23), calls=%async_computation.3 | async-start | bytes 131072 | tf_op jit(solution)/shard_map/all_to_all | solution.py:15
  142.4 14.5 %all-to-all-start.4 = ((bf16[8,128,128]{2,1,0:T(8,128)(2,1)}), bf16[8,128,128]{2,1,0:T(8,128)(2,1)S(1)}, u32[]{:S(2)}, u32[]{:S(2)}) async-start(bf16[8,128,128]{2,1,0:T(8,128)(2,1)} %broadcast_in_dim.24), calls=%async_computation.4 | async-start | bytes 524288 | tf_op jit(solution)/shard_map/all_to_all | solution.py:15
  157.6 8.1 %all-to-all-start.5 = ((bf16[4,128,128]{2,1,0:T(8,128)(2,1)}), bf16[4,128,128]{2,1,0:T(8,128)(2,1)S(1)}, u32[]{:S(2)}, u32[]{:S(2)}) async-start(bf16[4,128,128]{2,1,0:T(8,128)(2,1)} %broadcast_in_dim.27), calls=%async_computation.5 | async-start | bytes 262144 | tf_op jit(solution)/shard_map/all_to_all | solution.py:15
  198.7 33.0 %all-to-all-start.7 = ((bf16[8,16,352]{2,1,0:T(8,128)(2,1)}), bf16[8,16,352]{2,1,0:T(8,128)(2,1)S(1)}, u32[]{:S(2)}, u32[]{:S(2)}) async-start(bf16[8,16,352]{2,1,0:T(8,128)(2,1)} %broadcast_in_dim.29), calls=%async_computation.7 | async-start | bytes 196608 | tf_op jit(solution)/shard_map/all_to_all | solution.py:15
  232.7 18.2 %all-to-all-start.8 = ((bf16[32,16,128]{2,1,0:T(8,128)(2,1)}), bf16[32,16,128]{2,1,0:T(8,128)(2,1)S(1)}, u32[]{:S(2)}, u32[]{:S(2)}) async-start(bf16[32,16,128]{2,1,0:T(8,128)(2,1)} %bitcast.28), calls=%async_computation.8 | async-start | bytes 262144 | tf_op jit(solution)/shard_map/all_to_all | solution.py:15

commit v4 on v3

--- a/solution.py
+++ b/solution.py
@@ -31,13 +31,15 @@
     return lax.dynamic_index_in_dim(stack, index, 0, keepdims=False)
 
 
+together = lax.optimization_barrier
+
+
 def exchanged(stack, place, groups):
     got = [pick(stack, place)]
     for k in range(1, NEAR):
         pairs = [(g[i], g[i ^ k]) for g in groups for i in range(NEAR)]
         got.append(lax.ppermute(pick(stack, place ^ k), "kv", pairs))
-    got = jnp.stack(got)
-    return jnp.stack([pick(got, j ^ place) for j in range(NEAR)])
+    return got
 
 
 def step(
@@ -77,23 +79,25 @@
         both = jnp.concatenate([cut(w_gate, j), cut(w_up, j), ffn_gain[:, None], pad], axis=1)
         blocks = [both[:, at : at + 128] for at in range(0, width, 128)]
         pieces.append(jnp.concatenate(blocks + [w_down[j * units : (j + 1) * units]], axis=0))
-    got = exchanged(jnp.stack(pieces), place, near_groups)
-    at_down = width // 128 * rows
-    w_out = got[:, at_down:]
-    w_gate_up = jnp.concatenate(
-        [got[:, at : at + rows].reshape(-1, 128) for at in range(0, at_down, rows)], axis=1
-    )
+    pieces = jnp.stack(pieces)
 
     block = share(tokens.T, "tp", tp).reshape(-1, batch)
+    weights = jnp.concatenate([w_query, w_forget, w_input, w_outgate], axis=1)
+    own_at = (lax.axis_index("tp") * own_width).astype(jnp.uint32)
+    is_square = lax.iota(jnp.int32, width) == 2 * units
+    block, pieces, weights, lower_bound, head_gain, own_at, is_square = together(
+        (block, pieces, weights, lower_bound, head_gain.astype(f32), own_at, is_square)
+    )
     block_f = block.astype(f32)
     normed = (block_f * mix_gain.astype(f32)[:, None]).astype(bf16)
     squares = jnp.sum(block_f * block_f, axis=0)
-    weights = jnp.concatenate([w_query, w_forget, w_input, w_outgate], axis=1)
-    terms = dot_t(normed, lax.optimization_barrier(weights), ((0,), (0,))).astype(bf16)
+    terms = dot_t(normed, weights, ((0,), (0,))).astype(bf16)
     side = jnp.broadcast_to(squares.astype(bf16)[:, None], (batch, 128))
     terms = jnp.concatenate([terms, side], axis=1)
     terms = terms.reshape(far, NEAR, rows_here, -1).transpose(1, 0, 2, 3)
     terms = summed(spread(terms, "kv", near_groups)).astype(bf16)
+    terms, place = together((terms, place))
+    got = exchanged(pieces, place, near_groups)
     sums = spread(terms, "kv", far_groups)
     sums = summed(sums)
     key_width = heads_here * head_size
@@ -112,21 +116,31 @@
     new_state = forget[..., None] * state + key_in[..., None] * raw[2][:, :, None, :]
     readout = jnp.sum(query_act[..., None] * new_state, axis=2)
     head_rms = lax.rsqrt(jnp.mean(readout * readout, axis=-1, keepdims=True) + eps)
-    gated = readout * head_rms * head_gain.astype(f32) * jax.nn.silu(raw[3])
+    gated = readout * head_rms * head_gain * jax.nn.silu(raw[3])
     gated = gated.reshape(rows_here, key_width).astype(bf16)
+
+    gated, got[0] = together((gated, got[0]))
+    got = jnp.stack(got)
+    got = jnp.stack([pick(got, j ^ place) for j in range(NEAR)])
+    at_down = width // 128 * rows
+    w_out = got[:, at_down:]
+    w_gate_up = jnp.concatenate(
+        [got[:, at : at + rows].reshape(-1, 128) for at in range(0, at_down, rows)], axis=1
+    )
+    gain = w_gate_up[:, 2 * units : 2 * units + 1].astype(f32)
 
     gated_all = share(gated, "kv", kv).reshape(batch, key_width)
     mix = dot_t(w_mixout, gated_all, ((0,), (1,))).astype(bf16)
+    mix, w_gate_up, w_out, gain = together((mix, w_gate_up, w_out, gain))
     resid = (block_f + summed(share(mix, "tp", tp))).astype(bf16)
-    resid_own = lax.dynamic_slice_in_dim(resid, lax.axis_index("tp") * own_width, own_width, 0)
+    resid_own = lax.dynamic_slice(resid, (own_at, jnp.uint32(0)), (own_width, batch))
+    resid, resid_own = together((resid, resid_own))
 
     resid_f = share(resid, "kv", NEAR, near_groups).reshape(-1, batch).astype(f32)
-    gain = w_gate_up[:, 2 * units : 2 * units + 1].astype(f32)
     normed_ffn = (resid_f * gain).astype(bf16)
     squares_ffn = jnp.sum(resid_f * resid_f, axis=0)
     terms = dot_t(normed_ffn, w_gate_up, ((0,), (0,)))
-    column = lax.broadcasted_iota(jnp.int32, terms.shape, 1)
-    terms = jnp.where(column == 2 * units, squares_ffn[:, None], terms).astype(bf16)
+    terms = jnp.where(is_square, squares_ffn[:, None], terms).astype(bf16)
     sums = summed(spread(terms.reshape(far, -1, width), "kv", far_groups))
     inv_rms = lax.rsqrt(sums[:, 2 * units : 2 * units + 1] / D + eps)
     gate_sum, up_sum = sums[:, :units] * inv_rms, sums[:, units : 2 * units] * inv_rms

time: 253 us -> 256 us (1.012)
  blocking collectives: 31.5 us -> 102 us
  waiting for transfers between devices: 87.7 us -> 49.2 us
  starting transfers between devices: 114 us -> 86.6 us
    all_to_all x1 -> x5, blocking collectives: 31.5 us -> 102 us  [spread(): lax.all_to_all(parts, axis, 0, 0, axis_index_groups=groups, tiled=True)]
    all_to_all x8 -> x4, waiting for transfers between devices: 87.7 us -> 44 us  [spread(): lax.all_to_all(parts, axis, 0, 0, axis_index_groups=groups, tiled=True)]
    all_to_all x8 -> x4, starting transfers between devices: 104 us -> 77.3 us  [spread(): lax.all_to_all(parts, axis, 0, 0, axis_index_groups=groups, tiled=True)]
    ppermute x3, waiting for transfers between devices: 0.01 us -> 5.16 us  [exchanged(): got.append(lax.ppermute(pick(stack, place ^ k), 'kv', pairs))]
  transfers between devices with their start and end apart: 11 -> 7, of which waited for: 6 -> 4; matrix products, arithmetic and copies ran while one was open for 4% -> 3% of each run, Pallas kernels for 0% -> 0%
where the time goes in v4:
time: 256 us
  blocking collectives  102 us (40%)
  starting transfers between devices  86.6 us (34%)
  waiting for transfers between devices  49.2 us (19%)
  local copies, waits for them, and re-layouts  9.6 us (4%)
  other arithmetic  5.55 us (2%)
    all_to_all x5, blocking collectives, spread(): lax.all_to_all(parts, axis, 0, 0, axis_index_groups=groups, tiled=True)  102 us
    all_to_all x4, starting transfers between devices, spread(): lax.all_to_all(parts, axis, 0, 0, axis_index_groups=groups, tiled=True)  77.3 us
    all_to_all x4, waiting for transfers between devices, spread(): lax.all_to_all(parts, axis, 0, 0, axis_index_groups=groups, tiled=True)  44 us
    ppermute x3, starting transfers between devices, exchanged(): got.append(lax.ppermute(pick(stack, place ^ k), 'kv', pairs))  9.35 us
    ppermute x3, waiting for transfers between devices, exchanged(): got.append(lax.ppermute(pick(stack, place ^ k), 'kv', pairs))  5.16 us
  transfers between devices with their start and end apart: 7, of which 4 were waited for; matrix products, arithmetic and copies ran while one was open for 3% of the time, Pallas kernels for 0%

profile of v4, /device:TPU:33, one launch (start us, length us, event | category | flops | bytes accessed | tf_op | source)
XLA Modules:
  0.0 255.6 jit_solution(1933199892888851039)
XLA Ops:
  0.7 1.4 broadcast_in_dim.24
  2.0 44.7 %all-to-all-start = ((bf16[8,16,128]{2,1,0:T(8,128)(2,1)}), bf16[8,16,128]{2,1,0:T(8,128)(2,1)S(1)}, u32[]{:S(2)}, u32[]{:S(2)}) async-start(bf16[8,16,128]{2,1,0:T(8,128)(2,1)} %broadcast_in_dim.24), calls=%async_computation | async-start | bytes 65536 | tf_op jit(solution)/shard_map/all_to_all | solution.py:15
  46.7 1.0 constant_dynamic-update-slice_fusion.5
  47.7 1.2 fusion.23
  48.9 0.2 fusion.24
  49.1 0.1 copy.126
  49.2 0.1 pad_slice_fusion
  49.3 1.1 constant_dynamic-update-slice_fusion.4
  50.4 0.9 constant_dynamic-update-slice_fusion.15
  51.4 0.1 constant_dynamic-update-slice_fusion.21
  51.5 0.1 constant_dynamic-update-slice_fusion.3
  51.6 0.1 constant_dynamic-update-slice_fusion.2
  51.7 0.1 constant_dynamic-update-slice_fusion.1
  51.8 0.1 constant_dynamic-update-slice_fusion
  52.0 0.1 slice_dynamic-update-slice_fusion.3
  52.1 0.1 pad_maximum_fusion
  52.2 0.6 copy-done.4
  52.9 0.0 copy-done.6
  53.1 0.3 convolution_convert_fusion
  53.4 0.1 broadcast_in_dim.27
  53.5 0.1 reshape.122
  53.6 0.8 copy.154
  54.4 3.5 %all-to-all-start.1 = ((bf16[4,8,4,1152]{3,2,1,0:T(4,128)(2,1)}), bf16[4,8,4,1152]{3,2,1,0:T(4,128)(2,1)S(1)}, u32[]{:S(2)}, u32[]{:S(2)}) async-start(bf16[4,8,4,1152]{3,2,1,0:T(4,128)(2,1)} %bitcast.60), calls=%async_computation.1 | async-start | bytes 589824 | tf_op jit(solution)/shard_map/all_to_all | solution.py:15
  58.0 8.3 %all-to-all-done.1 = bf16[4,8,4,1152]{3,2,1,0:T(4,128)(2,1)S(1)} async-done(((bf16[4,8,4,1152]{3,2,1,0:T(4,128)(2,1)}), bf16[4,8,4,1152]{3,2,1,0:T(4,128)(2,1)S(1)}, u32[]{:S(2)}, u32[]{:S(2)}) %all-to-all-start.1) | async-done | bytes 294944 | tf_op jit(solution)/shard_map/all_to_all | solution.py:15
  66.3 0.8 reduce_sum.85
  67.1 6.6 %all-to-all-start.2 = ((bf16[8,4,1152]{2,1,0:T(4,128)(2,1)}), bf16[8,4,1152]{2,1,0:T(4,128)(2,1)S(1)}, u32[]{:S(2)}, u32[]{:S(2)}) async-start(bf16[8,4,1152]{2,1,0:T(4,128)(2,1)} %reduce_sum.85), calls=%async_computation.2 | async-start | bytes 147456 | tf_op jit(solution)/shard_map/all_to_all | solution.py:15
  73.8 0.8 dynamic-slice_bitcast_fusion.2
  74.6 2.4 collective-permute-start
  77.0 3.8 %collective-permute-start.1 = (bf16[1120,128]{1,0:T(8,128)(2,1)S(1)}, bf16[1120,128]{1,0:T(8,128)(2,1)S(1)}, u32[]{:S(2)}, u32[]{:S(2)}) collective-permute-start(bf16[1120,128]{1,0:T(8,128)(2,1)S(1)} %get-tuple-element.50), channel_id=1, source_target_pairs={{0,16},{8,24},{16,0},{24,8},{32,48},{40,56},{48,32},{56,40},{64,80... | collective-permute-start | bytes 860168 | tf_op jit(solution)/shard_map/ppermute | solution.py:41
  80.8 3.1 %collective-permute-start.2 = (bf16[1120,128]{1,0:T(8,128)(2,1)S(1)}, bf16[1120,128]{1,0:T(8,128)(2,1)S(1)}, u32[]{:S(2)}, u32[]{:S(2)}) collective-permute-start(bf16[1120,128]{1,0:T(8,128)(2,1)S(1)} %get-tuple-element.49), channel_id=1, source_target_pairs={{0,24},{8,16},{16,8},{24,0},{32,56},{40,48},{48,40},{56,32},{64,88... | collective-permute-start | bytes 860168 | tf_op jit(solution)/shard_map/ppermute | solution.py:41
  83.9 13.2 %all-to-all-done.2 = bf16[8,4,1152]{2,1,0:T(4,128)(2,1)S(1)} async-done(((bf16[8,4,1152]{2,1,0:T(4,128)(2,1)}), bf16[8,4,1152]{2,1,0:T(4,128)(2,1)S(1)}, u32[]{:S(2)}, u32[]{:S(2)}) %all-to-all-start.2) | async-done | bytes 73760 | tf_op jit(solution)/shard_map/all_to_all | solution.py:15
  97.1 0.1 convert_reduce_fusion.3
  97.1 0.1 fusion.22
  97.3 0.1 add_divide_fusion.1
  97.5 1.3 multiply_reduce_fusion
  98.7 0.1 multiply_reduce_fusion.2
  98.8 0.1 multiply_bitcast_fusion
  98.9 0.1 fusion.19
  99.0 5.2 %collective-permute-done.1 = bf16[1120,128]{1,0:T(8,128)(2,1)S(1)} collective-permute-done((bf16[1120,128]{1,0:T(8,128)(2,1)S(1)}, bf16[1120,128]{1,0:T(8,128)(2,1)S(1)}, u32[]{:S(2)}, u32[]{:S(2)}) %collective-permute-start.1) | collective-permute-done | bytes 286752 | tf_op jit(solution)/shard_map/ppermute | solution.py:41
  104.2 0.1 pad_maximum_fusion.1
  104.3 0.1 constant_dynamic-slice_fusion.3
  104.5 0.1 copy.143
  104.6 0.1 copy.141
  104.8 0.1 copy.142
  104.9 0.1 copy.144
  105.0 0.1 copy.145
  105.1 0.6 broadcast_in_dim.28
  105.8 22.4 %all-to-all-start.3 = ((bf16[32,4,256]{2,1,0:T(4,128)(2,1)}), bf16[32,4,256]{2,1,0:T(4,128)(2,1)S(1)}, u32[]{:S(2)}, u32[]{:S(2)}) async-start(bf16[32,4,256]{2,1,0:T(4,128)(2,1)} %broadcast_in_dim.28), calls=%async_computation.3 | async-start | bytes 131072 | tf_op jit(solution)/shard_map/all_to_all | solution.py:15
  128.3 0.1 copy.146
  128.5 22.5 %all-to-all-done.3 = bf16[32,4,256]{2,1,0:T(4,128)(2,1)S(1)} async-done(((bf16[32,4,256]{2,1,0:T(4,128)(2,1)}), bf16[32,4,256]{2,1,0:T(4,128)(2,1)S(1)}, u32[]{:S(2)}, u32[]{:S(2)}) %all-to-all-start.3) | async-done | bytes 65568 | tf_op jit(solution)/shard_map/all_to_all | solution.py:15
  151.0 0.1 fusion.1
  151.2 0.1 copy.138
  151.3 13.4 %all_to_all.45 = bf16[8,128,128]{2,1,0:T(8,128)(2,1)S(1)} all-to-all(bf16[8,128,128]{2,1,0:T(8,128)(2,1)S(1)} %broadcast_in_dim.29), channel_id=1, replica_groups=mesh['grp'=2,'kv'=32,'tp'=8] {'tp'}, dimensions={0} | all-to-all | bytes 524288 | tf_op jit(solution)/shard_map/all_to_all | solution.py:15
  164.9 7.2 %all_to_all.46 = bf16[4,128,128]{2,1,0:T(8,128)(2,1)S(1)} all-to-all(bf16[4,128,128]{2,1,0:T(8,128)(2,1)S(1)} %broadcast_in_dim.31), channel_id=1, replica_groups={{0,8,16,24},{32,40,48,56},{64,72,80,88},{96,104,112,120},{128,136,144,1..., dimensions={0} | all-to-all | bytes 262144 | tf_op jit(solution)/shard_map/all_to_all | solution.py:15
  172.1 0.1 multiply_reduce_fusion.1
  172.2 0.1 fusion.2
  172.3 0.4 fusion
  172.7 32.2 %all_to_all.47 = bf16[8,16,768]{2,1,0:T(8,128)(2,1)S(1)} all-to-all(bf16[8,16,768]{2,1,0:T(8,128)(2,1)S(1)} %bitcast.68), channel_id=1, replica_groups={{0,32,64,96,128,160,192,224},{8,40,72,104,136,168,200,232},{16,48,80,11..., dimensions={0} | all-to-all | bytes 393216 | tf_op jit(solution)/shard_map/all_to_all | solution.py:15
  204.9 0.2 fusion.16
  205.1 0.1 fusion.13
  205.2 33.4 %all_to_all.48 = bf16[8,16,352]{2,1,0:T(8,128)(2,1)S(1)} all-to-all(bf16[8,16,352]{2,1,0:T(8,128)(2,1)S(1)} %broadcast_in_dim.33), channel_id=1, replica_groups={{0,32,64,96,128,160,192,224},{8,40,72,104,136,168,200,232},{16,48,80,11..., dimensions={0} | all-to-all | bytes 180224 | tf_op jit(solution)/shard_map/all_to_all | solution.py:15
  238.6 0.3 convolution_convert_fusion.1
  238.9 16.1 %all_to_all.49 = bf16[32,16,128]{2,1,0:T(8,128)(2,1)S(1)} all-to-all(bf16[32,16,128]{2,1,0:T(8,128)(2,1)S(1)} %bitcast.76), channel_id=1, replica_groups={{0,1,2,3,4,5,6,7,8,9,10,11,12,13,14,15,16,17,18,19,20,21,22,23,24,25,26..., dimensions={0} | all-to-all | bytes 262144 | tf_op jit(solution)/shard_map/all_to_all | solution.py:15
  255.0 0.6 fusion.18
  (62 shorter events, 0.7 us)
Async XLA Ops:
  0.6 150.4 %copy-start = (bf16[256,128]{1,0:T(8,128)(2,1)S(1)}, bf16[256,128]{1,0:T(8,128)(2,1)}, u32[]{:S(2)}) copy-start(bf16[256,128]{1,0:T(8,128)(2,1)} %param.23) | copy-start | bytes 196612
  0.6 48.3 %copy-start.1 = (bf16[128,1408]{1,0:T(8,128)(2,1)S(1)}, bf16[128,1408]{1,0:T(8,128)(2,1)}, u32[]{:S(2)}) copy-start(bf16[128,1408]{1,0:T(8,128)(2,1)} %param.26) | copy-start | bytes 1081348
  0.7 48.4 %copy-start.9 = (bf16[128]{0:T(256)(128)(2,1)S(1)}, bf16[128]{0:T(256)(128)(2,1)}, u32[]{:S(2)}) copy-start(bf16[128]{0:T(256)(128)(2,1)} %param.24) | copy-start | bytes 772
  2.0 51.0 %all-to-all-start = ((bf16[8,16,128]{2,1,0:T(8,128)(2,1)}), bf16[8,16,128]{2,1,0:T(8,128)(2,1)S(1)}, u32[]{:S(2)}, u32[]{:S(2)}) async-start(bf16[8,16,128]{2,1,0:T(8,128)(2,1)} %broadcast_in_dim.24), calls=%async_computation | async-start | bytes 65536 | tf_op jit(solution)/shard_map/all_to_all | solution.py:15
  49.3 2.6 %copy-start.3 = (bf16[1408,128]{1,0:T(8,128)(2,1)S(1)}, bf16[1408,128]{1,0:T(8,128)(2,1)}, u32[]{:S(2)}) copy-start(bf16[1408,128]{1,0:T(8,128)(2,1)} %param.27) | copy-start | bytes 1081348
  52.0 0.8 copy-start.4
  52.0 0.9 copy-start.5
  52.0 0.9 copy-start.6
  52.0 0.9 copy-start.7
  52.1 0.9 copy-start.10
  52.1 1.0 copy-start.11
  53.5 20.2 %copy-start.8 = (f32[256]{0:T(256)S(1)}, f32[256]{0:T(256)}, u32[]{:S(2)}) copy-start(f32[256]{0:T(256)} %param.20) | copy-start | bytes 3076
  54.4 11.9 %all-to-all-start.1 = ((bf16[4,8,4,1152]{3,2,1,0:T(4,128)(2,1)}), bf16[4,8,4,1152]{3,2,1,0:T(4,128)(2,1)S(1)}, u32[]{:S(2)}, u32[]{:S(2)}) async-start(bf16[4,8,4,1152]{3,2,1,0:T(4,128)(2,1)} %bitcast.60), calls=%async_computation.1 | async-start | bytes 589824 | tf_op jit(solution)/shard_map/all_to_all | solution.py:15
  67.1 30.0 %all-to-all-start.2 = ((bf16[8,4,1152]{2,1,0:T(4,128)(2,1)}), bf16[8,4,1152]{2,1,0:T(4,128)(2,1)S(1)}, u32[]{:S(2)}, u32[]{:S(2)}) async-start(bf16[8,4,1152]{2,1,0:T(4,128)(2,1)} %reduce_sum.85), calls=%async_computation.2 | async-start | bytes 147456 | tf_op jit(solution)/shard_map/all_to_all | solution.py:15
  73.8 23.7 %copy-start.2 = (f32[4,2,128,128]{3,2,1,0:T(8,128)S(1)}, f32[4,2,128,128]{3,2,1,0:T(8,128)}, u32[]{:S(2)}) copy-start(f32[4,2,128,128]{3,2,1,0:T(8,128)} %param.21) | copy-start | bytes 1572868
  74.6 24.5 %collective-permute-start = (bf16[1120,128]{1,0:T(8,128)(2,1)}, bf16[1120,128]{1,0:T(8,128)(2,1)S(1)}, u32[]{:S(2)}, u32[]{:S(2)}) collective-permute-start(bf16[1120,128]{1,0:T(8,128)(2,1)} %get-tuple-element.48), channel_id=1, source_target_pairs={{0,8},{8,0},{16,24},{24,16},{32,40},{40,32},{48,56},{56,48},{64,72... | collective-permute-start | bytes 860168 | tf_op jit(solution)/shard_map/ppermute | solution.py:41
  77.0 27.2 %collective-permute-start.1 = (bf16[1120,128]{1,0:T(8,128)(2,1)S(1)}, bf16[1120,128]{1,0:T(8,128)(2,1)S(1)}, u32[]{:S(2)}, u32[]{:S(2)}) collective-permute-start(bf16[1120,128]{1,0:T(8,128)(2,1)S(1)} %get-tuple-element.50), channel_id=1, source_target_pairs={{0,16},{8,24},{16,0},{24,8},{32,48},{40,56},{48,32},{56,40},{64,80... | collective-permute-start | bytes 860168 | tf_op jit(solution)/shard_map/ppermute | solution.py:41
  80.8 23.4 %collective-permute-start.2 = (bf16[1120,128]{1,0:T(8,128)(2,1)S(1)}, bf16[1120,128]{1,0:T(8,128)(2,1)S(1)}, u32[]{:S(2)}, u32[]{:S(2)}) collective-permute-start(bf16[1120,128]{1,0:T(8,128)(2,1)S(1)} %get-tuple-element.49), channel_id=1, source_target_pairs={{0,24},{8,16},{16,8},{24,0},{32,56},{40,48},{48,40},{56,32},{64,88... | collective-permute-start | bytes 860168 | tf_op jit(solution)/shard_map/ppermute | solution.py:41
  105.8 45.2 %all-to-all-start.3 = ((bf16[32,4,256]{2,1,0:T(4,128)(2,1)}), bf16[32,4,256]{2,1,0:T(4,128)(2,1)S(1)}, u32[]{:S(2)}, u32[]{:S(2)}) async-start(bf16[32,4,256]{2,1,0:T(4,128)(2,1)} %broadcast_in_dim.28), calls=%async_computation.3 | async-start | bytes 131072 | tf_op jit(solution)/shard_map/all_to_all | solution.py:15

commit v5 on v4

--- a/solution.py
+++ b/solution.py
@@ -71,22 +71,14 @@
 
     units = w_gate.shape[1] // NEAR
     width = -(-(2 * units + 1) // 128) * 128
-    pad = jnp.zeros((w_gate.shape[0], width - 2 * units - 1), bf16)
-    cut = lambda w, j: w[:, j * units : (j + 1) * units]
     rows = w_gate.shape[0]
-    pieces = []
-    for j in range(NEAR):
-        both = jnp.concatenate([cut(w_gate, j), cut(w_up, j), ffn_gain[:, None], pad], axis=1)
-        blocks = [both[:, at : at + 128] for at in range(0, width, 128)]
-        pieces.append(jnp.concatenate(blocks + [w_down[j * units : (j + 1) * units]], axis=0))
-    pieces = jnp.stack(pieces)
 
     block = share(tokens.T, "tp", tp).reshape(-1, batch)
     weights = jnp.concatenate([w_query, w_forget, w_input, w_outgate], axis=1)
     own_at = (lax.axis_index("tp") * own_width).astype(jnp.uint32)
     is_square = lax.iota(jnp.int32, width) == 2 * units
-    block, pieces, weights, lower_bound, head_gain, own_at, is_square = together(
-        (block, pieces, weights, lower_bound, head_gain.astype(f32), own_at, is_square)
+    block, weights, lower_bound, head_gain, own_at, is_square = together(
+        (block, weights, lower_bound, head_gain.astype(f32), own_at, is_square)
     )
     block_f = block.astype(f32)
     normed = (block_f * mix_gain.astype(f32)[:, None]).astype(bf16)
@@ -95,8 +87,19 @@
     side = jnp.broadcast_to(squares.astype(bf16)[:, None], (batch, 128))
     terms = jnp.concatenate([terms, side], axis=1)
     terms = terms.reshape(far, NEAR, rows_here, -1).transpose(1, 0, 2, 3)
-    terms = summed(spread(terms, "kv", near_groups)).astype(bf16)
-    terms, place = together((terms, place))
+    terms = spread(terms, "kv", near_groups)
+
+    pad = jnp.zeros((rows, width - 2 * units - 1), bf16)
+    cut = lambda w, j: w[:, j * units : (j + 1) * units]
+    pieces = []
+    for j in range(NEAR):
+        both = jnp.concatenate([cut(w_gate, j), cut(w_up, j), ffn_gain[:, None], pad], axis=1)
+        blocks = [both[:, at : at + 128] for at in range(0, width, 128)]
+        pieces.append(jnp.concatenate(blocks + [w_down[j * units : (j + 1) * units]], axis=0))
+    pieces = jnp.stack(pieces)
+
+    terms, pieces, place = together((terms, pieces, place))
+    terms = summed(terms).astype(bf16)
     got = exchanged(pieces, place, near_groups)
     sums = spread(terms, "kv", far_groups)
     sums = summed(sums)
@@ -113,13 +116,14 @@
     bounds = lower_bound.reshape(heads_here, head_size)
     forget = bounds + (1.0 - bounds) * jax.nn.sigmoid(raw[1])
     key_in = (1.0 - bounds) * jax.nn.sigmoid(-raw[1])
-    new_state = forget[..., None] * state + key_in[..., None] * raw[2][:, :, None, :]
-    readout = jnp.sum(query_act[..., None] * new_state, axis=2)
+    from_state = jnp.sum((query_act * forget)[..., None] * state, axis=2)
+    readout = from_state + jnp.sum(query_act * key_in, axis=-1, keepdims=True) * raw[2]
     head_rms = lax.rsqrt(jnp.mean(readout * readout, axis=-1, keepdims=True) + eps)
     gated = readout * head_rms * head_gain * jax.nn.silu(raw[3])
     gated = gated.reshape(rows_here, key_width).astype(bf16)
 
-    gated, got[0] = together((gated, got[0]))
+    gated, got[0], forget, key_in, values_in = together((gated, got[0], forget, key_in, raw[2]))
+    new_state = forget[..., None] * state + key_in[..., None] * values_in[:, :, None, :]
     got = jnp.stack(got)
     got = jnp.stack([pick(got, j ^ place) for j in range(NEAR)])
     at_down = width // 128 * rows
@@ -131,7 +135,7 @@
 
     gated_all = share(gated, "kv", kv).reshape(batch, key_width)
     mix = dot_t(w_mixout, gated_all, ((0,), (1,))).astype(bf16)
-    mix, w_gate_up, w_out, gain = together((mix, w_gate_up, w_out, gain))
+    mix, w_gate_up, w_out, gain, new_state = together((mix, w_gate_up, w_out, gain, new_state))
     resid = (block_f + summed(share(mix, "tp", tp))).astype(bf16)
     resid_own = lax.dynamic_slice(resid, (own_at, jnp.uint32(0)), (own_width, batch))
     resid, resid_own = together((resid, resid_own))

time: 256 us -> 254 us (level)
  waiting for transfers between devices: 49.2 us -> 46.1 us
    all_to_all x4, waiting for transfers between devices: 44 us -> 40.2 us  [spread(): lax.all_to_all(parts, axis, 0, 0, axis_index_groups=groups, tiled=True)]
  transfers between devices with their start and end apart: 7 -> 7, of which waited for: 4 -> 5; matrix products, arithmetic and copies ran while one was open for 3% -> 3% of each run, Pallas kernels for 0% -> 0%
where the time goes in v5:
time: 254 us; the launch traced here: 253 us
  blocking collectives  102 us (40%)
  starting transfers between devices  87.7 us (35%)
  waiting for transfers between devices  46.1 us (18%)
  local copies, waits for them, and re-layouts  9.05 us (4%)
  other arithmetic  5.72 us (2%)
    all_to_all x5, blocking collectives, spread(): lax.all_to_all(parts, axis, 0, 0, axis_index_groups=groups, tiled=True)  102 us
    all_to_all x4, starting transfers between devices, spread(): lax.all_to_all(parts, axis, 0, 0, axis_index_groups=groups, tiled=True)  78.3 us
    all_to_all x4, waiting for transfers between devices, spread(): lax.all_to_all(parts, axis, 0, 0, axis_index_groups=groups, tiled=True)  40.2 us
    ppermute x3, starting transfers between devices, exchanged(): got.append(lax.ppermute(pick(stack, place ^ k), 'kv', pairs))  9.35 us
    ppermute x3, waiting for transfers between devices, exchanged(): got.append(lax.ppermute(pick(stack, place ^ k), 'kv', pairs))  5.94 us
  transfers between devices with their start and end apart: 7, of which 5 were waited for; matrix products, arithmetic and copies ran while one was open for 3% of the time, Pallas kernels for 0%

profile of v5, /device:TPU:33, one launch (start us, length us, event | category | flops | bytes accessed | tf_op | source)
XLA Modules:
  0.0 253.3 jit_solution(18139214531485168936)
XLA Ops:
  0.7 1.4 broadcast_in_dim.24
  2.1 44.7 %all-to-all-start = ((bf16[8,16,128]{2,1,0:T(8,128)(2,1)}), bf16[8,16,128]{2,1,0:T(8,128)(2,1)S(1)}, u32[]{:S(2)}, u32[]{:S(2)}) async-start(bf16[8,16,128]{2,1,0:T(8,128)(2,1)} %broadcast_in_dim.24), calls=%async_computation | async-start | bytes 65536 | tf_op jit(solution)/shard_map/all_to_all | solution.py:15
  46.8 1.0 constant_dynamic-update-slice_fusion.5
  47.8 1.2 fusion.26
  49.0 0.2 fusion.27
  49.3 2.2 all-to-all-done
  51.6 0.3 convolution_convert_fusion
  51.9 0.1 broadcast_in_dim.25
  52.0 0.1 reshape.121
  52.1 0.8 copy.186
  52.9 3.5 %all-to-all-start.1 = ((bf16[4,8,4,1152]{3,2,1,0:T(4,128)(2,1)}), bf16[4,8,4,1152]{3,2,1,0:T(4,128)(2,1)S(1)}, u32[]{:S(2)}, u32[]{:S(2)}) async-start(bf16[4,8,4,1152]{3,2,1,0:T(4,128)(2,1)} %bitcast.77), calls=%async_computation.1 | async-start | bytes 589824 | tf_op jit(solution)/shard_map/all_to_all | solution.py:15
  56.5 1.0 constant_dynamic-update-slice_fusion.4
  57.5 0.1 copy.151
  57.7 0.1 pad_slice_fusion
  57.8 0.9 constant_dynamic-update-slice_fusion.15
  58.7 0.1 constant_dynamic-update-slice_fusion.21
  58.8 0.1 constant_dynamic-update-slice_fusion.3
  58.9 0.1 constant_dynamic-update-slice_fusion.2
  59.0 0.1 constant_dynamic-update-slice_fusion.1
  59.2 0.1 constant_dynamic-update-slice_fusion
  59.4 0.1 pad_maximum_fusion
  59.5 4.9 %all-to-all-done.1 = bf16[4,8,4,1152]{3,2,1,0:T(4,128)(2,1)S(1)} async-done(((bf16[4,8,4,1152]{3,2,1,0:T(4,128)(2,1)}), bf16[4,8,4,1152]{3,2,1,0:T(4,128)(2,1)S(1)}, u32[]{:S(2)}, u32[]{:S(2)}) %all-to-all-start.1) | async-done | bytes 294944 | tf_op jit(solution)/shard_map/all_to_all | solution.py:15
  64.4 0.8 reduce_sum.96
  65.2 6.5 %all-to-all-start.2 = ((bf16[8,4,1152]{2,1,0:T(4,128)(2,1)}), bf16[8,4,1152]{2,1,0:T(4,128)(2,1)S(1)}, u32[]{:S(2)}, u32[]{:S(2)}) async-start(bf16[8,4,1152]{2,1,0:T(4,128)(2,1)} %reduce_sum.96), calls=%async_computation.2 | async-start | bytes 147456 | tf_op jit(solution)/shard_map/all_to_all | solution.py:15
  71.8 0.9 dynamic-slice_bitcast_fusion.2
  72.7 1.9 collective-permute-start
  74.6 4.3 %collective-permute-start.1 = (bf16[1120,128]{1,0:T(8,128)(2,1)}, bf16[1120,128]{1,0:T(8,128)(2,1)S(1)}, u32[]{:S(2)}, u32[]{:S(2)}) collective-permute-start(bf16[1120,128]{1,0:T(8,128)(2,1)} %get-tuple-element.61), channel_id=1, source_target_pairs={{0,16},{8,24},{16,0},{24,8},{32,48},{40,56},{48,32},{56,40},{64,80... | collective-permute-start | bytes 860168 | tf_op jit(solution)/shard_map/ppermute | solution.py:41
  79.0 3.1 %collective-permute-start.2 = (bf16[1120,128]{1,0:T(8,128)(2,1)S(1)}, bf16[1120,128]{1,0:T(8,128)(2,1)S(1)}, u32[]{:S(2)}, u32[]{:S(2)}) collective-permute-start(bf16[1120,128]{1,0:T(8,128)(2,1)S(1)} %get-tuple-element.60), channel_id=1, source_target_pairs={{0,24},{8,16},{16,8},{24,0},{32,56},{40,48},{48,40},{56,32},{64,88... | collective-permute-start | bytes 860168 | tf_op jit(solution)/shard_map/ppermute | solution.py:41
  82.1 11.6 %all-to-all-done.2 = bf16[8,4,1152]{2,1,0:T(4,128)(2,1)S(1)} async-done(((bf16[8,4,1152]{2,1,0:T(4,128)(2,1)}), bf16[8,4,1152]{2,1,0:T(4,128)(2,1)S(1)}, u32[]{:S(2)}, u32[]{:S(2)}) %all-to-all-start.2) | async-done | bytes 73760 | tf_op jit(solution)/shard_map/all_to_all | solution.py:15
  93.6 0.1 convert_reduce_fusion.3
  93.7 0.1 fusion.24
  93.8 0.1 slice_multiply_fusion.4
  94.0 0.1 multiply_reduce_fusion.3
  94.1 0.2 multiply_reduce_fusion
  94.3 0.2 broadcast_bitcast_fusion.1
  94.5 0.1 broadcast_bitcast_fusion
  94.5 0.1 fusion.21
  94.7 5.9 %collective-permute-done.2 = bf16[1120,128]{1,0:T(8,128)(2,1)S(1)} collective-permute-done((bf16[1120,128]{1,0:T(8,128)(2,1)S(1)}, bf16[1120,128]{1,0:T(8,128)(2,1)S(1)}, u32[]{:S(2)}, u32[]{:S(2)}) %collective-permute-start.2) | collective-permute-done | bytes 286752 | tf_op jit(solution)/shard_map/ppermute | solution.py:41
  100.6 0.1 pad_maximum_fusion.1
  100.7 0.1 constant_dynamic-slice_fusion.3
  100.9 0.1 copy.167
  101.1 0.1 copy.165
  101.2 0.1 copy.166
  101.3 0.1 copy.168
  101.4 0.1 copy.169
  101.6 0.1 copy.170
  101.7 0.6 broadcast_in_dim.28
  102.3 23.6 %all-to-all-start.3 = ((bf16[32,4,256]{2,1,0:T(4,128)(2,1)}), bf16[32,4,256]{2,1,0:T(4,128)(2,1)S(1)}, u32[]{:S(2)}, u32[]{:S(2)}) async-start(bf16[32,4,256]{2,1,0:T(4,128)(2,1)} %broadcast_in_dim.28), calls=%async_computation.3 | async-start | bytes 131072 | tf_op jit(solution)/shard_map/all_to_all | solution.py:15
  126.0 1.1 multiply_add_fusion
  127.1 21.5 %all-to-all-done.3 = bf16[32,4,256]{2,1,0:T(4,128)(2,1)S(1)} async-done(((bf16[32,4,256]{2,1,0:T(4,128)(2,1)}), bf16[32,4,256]{2,1,0:T(4,128)(2,1)S(1)}, u32[]{:S(2)}, u32[]{:S(2)}) %all-to-all-start.3) | async-done | bytes 65568 | tf_op jit(solution)/shard_map/all_to_all | solution.py:15
  148.7 0.1 fusion.1
  148.8 0.1 copy.162
  149.0 12.9 %all_to_all.45 = bf16[8,128,128]{2,1,0:T(8,128)(2,1)S(1)} all-to-all(bf16[8,128,128]{2,1,0:T(8,128)(2,1)S(1)} %broadcast_in_dim.29), channel_id=1, replica_groups=mesh['grp'=2,'kv'=32,'tp'=8] {'tp'}, dimensions={0} | all-to-all | bytes 524288 | tf_op jit(solution)/shard_map/all_to_all | solution.py:15
  161.9 7.2 %all_to_all.46 = bf16[4,128,128]{2,1,0:T(8,128)(2,1)S(1)} all-to-all(bf16[4,128,128]{2,1,0:T(8,128)(2,1)S(1)} %broadcast_in_dim.31), channel_id=1, replica_groups={{0,8,16,24},{32,40,48,56},{64,72,80,88},{96,104,112,120},{128,136,144,1..., dimensions={0} | all-to-all | bytes 262144 | tf_op jit(solution)/shard_map/all_to_all | solution.py:15
  169.1 0.1 multiply_reduce_fusion.1
  169.2 0.1 fusion.2
  169.4 0.4 fusion
  169.8 32.2 %all_to_all.47 = bf16[8,16,768]{2,1,0:T(8,128)(2,1)S(1)} all-to-all(bf16[8,16,768]{2,1,0:T(8,128)(2,1)S(1)} %bitcast.85), channel_id=1, replica_groups={{0,32,64,96,128,160,192,224},{8,40,72,104,136,168,200,232},{16,48,80,11..., dimensions={0} | all-to-all | bytes 393216 | tf_op jit(solution)/shard_map/all_to_all | solution.py:15
  202.0 0.2 fusion.16
  202.2 0.1 fusion.13
  202.3 33.4 %all_to_all.48 = bf16[8,16,352]{2,1,0:T(8,128)(2,1)S(1)} all-to-all(bf16[8,16,352]{2,1,0:T(8,128)(2,1)S(1)} %broadcast_in_dim.33), channel_id=1, replica_groups={{0,32,64,96,128,160,192,224},{8,40,72,104,136,168,200,232},{16,48,80,11..., dimensions={0} | all-to-all | bytes 180224 | tf_op jit(solution)/shard_map/all_to_all | solution.py:15
  235.7 0.3 convolution_convert_fusion.1
  236.0 16.7 %all_to_all.49 = bf16[32,16,128]{2,1,0:T(8,128)(2,1)S(1)} all-to-all(bf16[32,16,128]{2,1,0:T(8,128)(2,1)S(1)} %bitcast.93), channel_id=1, replica_groups={{0,1,2,3,4,5,6,7,8,9,10,11,12,13,14,15,16,17,18,19,20,21,22,23,24,25,26..., dimensions={0} | all-to-all | bytes 262144 | tf_op jit(solution)/shard_map/all_to_all | solution.py:15
  252.7 0.6 fusion.18
  (63 shorter events, 0.7 us)
Async XLA Ops:
  0.6 148.0 %copy-start = (bf16[256,128]{1,0:T(8,128)(2,1)S(1)}, bf16[256,128]{1,0:T(8,128)(2,1)}, u32[]{:S(2)}) copy-start(bf16[256,128]{1,0:T(8,128)(2,1)} %param.23) | copy-start | bytes 196612
  0.6 48.4 %copy-start.2 = (bf16[128,1408]{1,0:T(8,128)(2,1)S(1)}, bf16[128,1408]{1,0:T(8,128)(2,1)}, u32[]{:S(2)}) copy-start(bf16[128,1408]{1,0:T(8,128)(2,1)} %param.26) | copy-start | bytes 1081348
  0.7 48.5 %copy-start.7 = (bf16[128,256]{1,0:T(8,128)(2,1)S(1)}, bf16[128,256]{1,0:T(8,128)(2,1)}, u32[]{:S(2)}) copy-start(bf16[128,256]{1,0:T(8,128)(2,1)} %param.16) | copy-start | bytes 196612
  0.7 48.5 %copy-start.6 = (bf16[128,256]{1,0:T(8,128)(2,1)S(1)}, bf16[128,256]{1,0:T(8,128)(2,1)}, u32[]{:S(2)}) copy-start(bf16[128,256]{1,0:T(8,128)(2,1)} %param.17) | copy-start | bytes 196612
  0.7 48.5 %copy-start.5 = (bf16[128,256]{1,0:T(8,128)(2,1)S(1)}, bf16[128,256]{1,0:T(8,128)(2,1)}, u32[]{:S(2)}) copy-start(bf16[128,256]{1,0:T(8,128)(2,1)} %param.18) | copy-start | bytes 196612
  0.7 48.5 %copy-start.4 = (bf16[128,256]{1,0:T(8,128)(2,1)S(1)}, bf16[128,256]{1,0:T(8,128)(2,1)}, u32[]{:S(2)}) copy-start(bf16[128,256]{1,0:T(8,128)(2,1)} %param.19) | copy-start | bytes 196612
  2.1 49.5 %all-to-all-start = ((bf16[8,16,128]{2,1,0:T(8,128)(2,1)}), bf16[8,16,128]{2,1,0:T(8,128)(2,1)S(1)}, u32[]{:S(2)}, u32[]{:S(2)}) async-start(bf16[8,16,128]{2,1,0:T(8,128)(2,1)} %broadcast_in_dim.24), calls=%async_computation | async-start | bytes 65536 | tf_op jit(solution)/shard_map/all_to_all | solution.py:15
  46.8 2.5 copy-start.10
  46.8 2.5 copy-start.11
  52.0 5.5 %copy-start.9 = (bf16[128]{0:T(256)(128)(2,1)S(1)}, bf16[128]{0:T(256)(128)(2,1)}, u32[]{:S(2)}) copy-start(bf16[128]{0:T(256)(128)(2,1)} %param.24) | copy-start | bytes 772
  52.9 11.5 %all-to-all-start.1 = ((bf16[4,8,4,1152]{3,2,1,0:T(4,128)(2,1)}), bf16[4,8,4,1152]{3,2,1,0:T(4,128)(2,1)S(1)}, u32[]{:S(2)}, u32[]{:S(2)}) async-start(bf16[4,8,4,1152]{3,2,1,0:T(4,128)(2,1)} %bitcast.77), calls=%async_computation.1 | async-start | bytes 589824 | tf_op jit(solution)/shard_map/all_to_all | solution.py:15
  57.5 1.8 copy-start.3
  59.4 12.4 %copy-start.8 = (f32[256]{0:T(256)S(1)}, f32[256]{0:T(256)}, u32[]{:S(2)}) copy-start(f32[256]{0:T(256)} %param.20) | copy-start | bytes 3076
  65.2 28.4 %all-to-all-start.2 = ((bf16[8,4,1152]{2,1,0:T(4,128)(2,1)}), bf16[8,4,1152]{2,1,0:T(4,128)(2,1)S(1)}, u32[]{:S(2)}, u32[]{:S(2)}) async-start(bf16[8,4,1152]{2,1,0:T(4,128)(2,1)} %reduce_sum.96), calls=%async_computation.2 | async-start | bytes 147456 | tf_op jit(solution)/shard_map/all_to_all | solution.py:15
  71.8 22.3 %copy-start.1 = (f32[4,2,128,128]{3,2,1,0:T(8,128)S(1)}, f32[4,2,128,128]{3,2,1,0:T(8,128)}, u32[]{:S(2)}) copy-start(f32[4,2,128,128]{3,2,1,0:T(8,128)} %param.21) | copy-start | bytes 1572868
  72.7 22.0 %collective-permute-start = (bf16[1120,128]{1,0:T(8,128)(2,1)}, bf16[1120,128]{1,0:T(8,128)(2,1)S(1)}, u32[]{:S(2)}, u32[]{:S(2)}) collective-permute-start(bf16[1120,128]{1,0:T(8,128)(2,1)} %get-tuple-element.59), channel_id=1, source_target_pairs={{0,8},{8,0},{16,24},{24,16},{32,40},{40,32},{48,56},{56,48},{64,72... | collective-permute-start | bytes 860168 | tf_op jit(solution)/shard_map/ppermute | solution.py:41
  74.6 20.0 %collective-permute-start.1 = (bf16[1120,128]{1,0:T(8,128)(2,1)}, bf16[1120,128]{1,0:T(8,128)(2,1)S(1)}, u32[]{:S(2)}, u32[]{:S(2)}) collective-permute-start(bf16[1120,128]{1,0:T(8,128)(2,1)} %get-tuple-element.61), channel_id=1, source_target_pairs={{0,16},{8,24},{16,0},{24,8},{32,48},{40,56},{48,32},{56,40},{64,80... | collective-permute-start | bytes 860168 | tf_op jit(solution)/shard_map/ppermute | solution.py:41
  79.0 21.6 %collective-permute-start.2 = (bf16[1120,128]{1,0:T(8,128)(2,1)S(1)}, bf16[1120,128]{1,0:T(8,128)(2,1)S(1)}, u32[]{:S(2)}, u32[]{:S(2)}) collective-permute-start(bf16[1120,128]{1,0:T(8,128)(2,1)S(1)} %get-tuple-element.60), channel_id=1, source_target_pairs={{0,24},{8,16},{16,8},{24,0},{32,56},{40,48},{48,40},{56,32},{64,88... | collective-permute-start | bytes 860168 | tf_op jit(solution)/shard_map/ppermute | solution.py:41
  102.3 46.3 %all-to-all-start.3 = ((bf16[32,4,256]{2,1,0:T(4,128)(2,1)}), bf16[32,4,256]{2,1,0:T(4,128)(2,1)S(1)}, u32[]{:S(2)}, u32[]{:S(2)}) async-start(bf16[32,4,256]{2,1,0:T(4,128)(2,1)} %broadcast_in_dim.28), calls=%async_computation.3 | async-start | bytes 131072 | tf_op jit(solution)/shard_map/all_to_all | solution.py:15

commit v6 on v5

--- a/solution.py
+++ b/solution.py
@@ -89,13 +89,19 @@
     terms = terms.reshape(far, NEAR, rows_here, -1).transpose(1, 0, 2, 3)
     terms = spread(terms, "kv", near_groups)
 
-    pad = jnp.zeros((rows, width - 2 * units - 1), bf16)
     cut = lambda w, j: w[:, j * units : (j + 1) * units]
+    whole = 2 * units // rows * rows
+    rest = 2 * units - whole
+    folds = rows // rest
+    gains = jnp.broadcast_to(ffn_gain[None], (16, rows))
     pieces = []
     for j in range(NEAR):
-        both = jnp.concatenate([cut(w_gate, j), cut(w_up, j), ffn_gain[:, None], pad], axis=1)
-        blocks = [both[:, at : at + 128] for at in range(0, width, 128)]
-        pieces.append(jnp.concatenate(blocks + [w_down[j * units : (j + 1) * units]], axis=0))
+        both = jnp.concatenate([cut(w_gate, j), cut(w_up, j)], axis=1)
+        blocks = [both[:, at : at + rows] for at in range(0, whole, rows)]
+        folded = both[:, whole:].reshape(folds, rest, rest)
+        blocks.append(jnp.concatenate([folded[i] for i in range(folds)], axis=1))
+        blocks += [w_down[j * units : (j + 1) * units], gains]
+        pieces.append(jnp.concatenate(blocks, axis=0))
     pieces = jnp.stack(pieces)
 
     terms, pieces, place = together((terms, pieces, place))
@@ -126,12 +132,14 @@
     new_state = forget[..., None] * state + key_in[..., None] * values_in[:, :, None, :]
     got = jnp.stack(got)
     got = jnp.stack([pick(got, j ^ place) for j in range(NEAR)])
-    at_down = width // 128 * rows
-    w_out = got[:, at_down:]
-    w_gate_up = jnp.concatenate(
-        [got[:, at : at + rows].reshape(-1, 128) for at in range(0, at_down, rows)], axis=1
-    )
-    gain = w_gate_up[:, 2 * units : 2 * units + 1].astype(f32)
+    folded = got[:, whole : whole + rest]
+    folded = [folded[..., i * rest : (i + 1) * rest] for i in range(folds)]
+    blocks = [got[:, at : at + rows].reshape(-1, rows) for at in range(0, whole, rows)]
+    blocks.append(jnp.concatenate(folded, axis=1).reshape(-1, rest))
+    blocks.append(jnp.zeros((NEAR * rows, width - 2 * units), bf16))
+    w_gate_up = jnp.concatenate(blocks, axis=1)
+    w_out = got[:, whole + rest : whole + rest + units]
+    gain = got[:, whole + rest + units].reshape(-1, 1).astype(f32)
 
     gated_all = share(gated, "kv", kv).reshape(batch, key_width)
     mix = dot_t(w_mixout, gated_all, ((0,), (1,))).astype(bf16)

time: 254 us -> 233 us (0.917)
  starting transfers between devices: 87.7 us -> 72.4 us
  waiting for transfers between devices: 46.1 us -> 40.9 us
    all_to_all x4, starting transfers between devices: 78.3 us -> 63.8 us  [spread(): lax.all_to_all(parts, axis, 0, 0, axis_index_groups=groups, tiled=True)]
    ppermute x3, waiting for transfers between devices: 5.94 us -> 0.87 us  [exchanged(): got.append(lax.ppermute(pick(stack, place ^ k), 'kv', pairs))]
  transfers between devices with their start and end apart: 7 -> 7, of which waited for: 5 -> 5; matrix products, arithmetic and copies ran while one was open for 3% -> 4% of each run, Pallas kernels for 0% -> 0%
where the time goes in v6:
time: 233 us
  blocking collectives  103 us (44%)
  starting transfers between devices  72.4 us (31%)
  waiting for transfers between devices  40.9 us (18%)
  local copies, waits for them, and re-layouts  7.73 us (3%)
  other arithmetic  6.05 us (3%)
    all_to_all x5, blocking collectives, spread(): lax.all_to_all(parts, axis, 0, 0, axis_index_groups=groups, tiled=True)  103 us
    all_to_all x4, starting transfers between devices, spread(): lax.all_to_all(parts, axis, 0, 0, axis_index_groups=groups, tiled=True)  63.8 us
    all_to_all x4, waiting for transfers between devices, spread(): lax.all_to_all(parts, axis, 0, 0, axis_index_groups=groups, tiled=True)  40.1 us
    ppermute x3, starting transfers between devices, exchanged(): got.append(lax.ppermute(pick(stack, place ^ k), 'kv', pairs))  8.6 us
  transfers between devices with their start and end apart: 7, of which 5 were waited for; matrix products, arithmetic and copies ran while one was open for 4% of the time, Pallas kernels for 0%

profile of v6, /device:TPU:33, one launch (start us, length us, event | category | flops | bytes accessed | tf_op | source)
XLA Modules:
  0.0 232.5 jit_solution(11904438565978234937)
XLA Ops:
  0.7 1.4 broadcast_in_dim.24
  2.0 44.7 %all-to-all-start = ((bf16[8,16,128]{2,1,0:T(8,128)(2,1)}), bf16[8,16,128]{2,1,0:T(8,128)(2,1)S(1)}, u32[]{:S(2)}, u32[]{:S(2)}) async-start(bf16[8,16,128]{2,1,0:T(8,128)(2,1)} %broadcast_in_dim.24), calls=%async_computation | async-start | bytes 65536 | tf_op jit(solution)/shard_map/all_to_all | solution.py:15
  46.7 1.0 fusion.39
  47.7 1.2 fusion.41
  49.0 0.2 fusion.40
  49.1 0.1 constant_dynamic-update-slice_fusion.6
  49.2 0.1 constant_dynamic-update-slice_fusion.5
  49.4 0.1 constant_dynamic-update-slice_fusion.18
  49.5 0.1 copy-done.12
  49.6 1.9 all-to-all-done
  51.5 0.3 convolution_convert_fusion
  51.8 0.1 broadcast_in_dim.25
  52.0 0.1 reshape.156
  52.1 0.8 copy.96
  52.9 3.7 %all-to-all-start.1 = ((bf16[4,8,4,1152]{3,2,1,0:T(4,128)(2,1)}), bf16[4,8,4,1152]{3,2,1,0:T(4,128)(2,1)S(1)}, u32[]{:S(2)}, u32[]{:S(2)}) async-start(bf16[4,8,4,1152]{3,2,1,0:T(4,128)(2,1)} %bitcast.81), calls=%async_computation.1 | async-start | bytes 589824 | tf_op jit(solution)/shard_map/all_to_all | solution.py:15
  56.6 0.1 constant_dynamic-update-slice_fusion.25
  56.7 0.1 constant_dynamic-update-slice_fusion.4
  56.8 0.1 constant_dynamic-update-slice_fusion.3
  56.9 0.1 constant_dynamic-update-slice_fusion.2
  57.0 0.1 constant_dynamic-update-slice_fusion.1
  57.1 0.1 constant_dynamic-update-slice_fusion.22
  57.2 0.1 constant_dynamic-update-slice_fusion.15
  57.3 0.1 constant_dynamic-update-slice_fusion.8
  57.5 0.1 pad_maximum_fusion
  57.6 6.9 %all-to-all-done.1 = bf16[4,8,4,1152]{3,2,1,0:T(4,128)(2,1)S(1)} async-done(((bf16[4,8,4,1152]{3,2,1,0:T(4,128)(2,1)}), bf16[4,8,4,1152]{3,2,1,0:T(4,128)(2,1)S(1)}, u32[]{:S(2)}, u32[]{:S(2)}) %all-to-all-start.1) | async-done | bytes 294944 | tf_op jit(solution)/shard_map/all_to_all | solution.py:15
  64.5 0.8 reduce_sum.96
  65.3 6.5 %all-to-all-start.2 = ((bf16[8,4,1152]{2,1,0:T(4,128)(2,1)}), bf16[8,4,1152]{2,1,0:T(4,128)(2,1)S(1)}, u32[]{:S(2)}, u32[]{:S(2)}) async-start(bf16[8,4,1152]{2,1,0:T(4,128)(2,1)} %reduce_sum.96), calls=%async_computation.2 | async-start | bytes 147456 | tf_op jit(solution)/shard_map/all_to_all | solution.py:15
  71.9 0.1 dynamic-slice_bitcast_fusion.2
  72.0 2.1 collective-permute-start
  74.1 4.1 %collective-permute-start.2 = (bf16[1072,128]{1,0:T(8,128)(2,1)S(1)}, bf16[1072,128]{1,0:T(8,128)(2,1)S(1)}, u32[]{:S(2)}, u32[]{:S(2)}) collective-permute-start(bf16[1072,128]{1,0:T(8,128)(2,1)S(1)} %get-tuple-element.59), channel_id=1, source_target_pairs={{0,24},{8,16},{16,8},{24,0},{32,56},{40,48},{48,40},{56,32},{64,88... | collective-permute-start | bytes 823304 | tf_op jit(solution)/shard_map/ppermute | solution.py:41
  78.1 2.4 %collective-permute-start.1 = (bf16[1072,128]{1,0:T(8,128)(2,1)S(1)}, bf16[1072,128]{1,0:T(8,128)(2,1)S(1)}, u32[]{:S(2)}, u32[]{:S(2)}) collective-permute-start(bf16[1072,128]{1,0:T(8,128)(2,1)S(1)} %get-tuple-element.60), channel_id=1, source_target_pairs={{0,16},{8,24},{16,0},{24,8},{32,48},{40,56},{48,32},{56,40},{64,80... | collective-permute-start | bytes 823304 | tf_op jit(solution)/shard_map/ppermute | solution.py:41
  80.6 13.2 %all-to-all-done.2 = bf16[8,4,1152]{2,1,0:T(4,128)(2,1)S(1)} async-done(((bf16[8,4,1152]{2,1,0:T(4,128)(2,1)}), bf16[8,4,1152]{2,1,0:T(4,128)(2,1)S(1)}, u32[]{:S(2)}, u32[]{:S(2)}) %all-to-all-start.2) | async-done | bytes 73760 | tf_op jit(solution)/shard_map/all_to_all | solution.py:15
  93.8 0.1 fusion.36
  93.9 0.1 slice_multiply_fusion.4
  94.1 0.1 multiply_reduce_fusion.3
  94.2 0.2 multiply_reduce_fusion
  94.4 0.2 broadcast_bitcast_fusion.1
  94.6 0.1 broadcast_bitcast_fusion
  94.7 0.1 fusion.32
  94.8 0.7 broadcast_in_dim.27
  95.4 9.0 %all-to-all-start.3 = ((bf16[32,4,256]{2,1,0:T(4,128)(2,1)}), bf16[32,4,256]{2,1,0:T(4,128)(2,1)S(1)}, u32[]{:S(2)}, u32[]{:S(2)}) async-start(bf16[32,4,256]{2,1,0:T(4,128)(2,1)} %broadcast_in_dim.27), calls=%async_computation.3 | async-start | bytes 131072 | tf_op jit(solution)/shard_map/all_to_all | solution.py:15
  104.4 0.9 collective-permute-done.1
  105.3 0.1 pad_maximum_fusion.1
  105.4 0.1 constant_dynamic-slice_fusion.3
  105.5 0.1 pad_maximum_fusion.2
  105.7 0.1 fusion.38
  105.8 0.9 fusion.14
  106.7 1.1 concatenate.63
  107.9 1.1 multiply_add_fusion
  109.0 18.1 %all-to-all-done.3 = bf16[32,4,256]{2,1,0:T(4,128)(2,1)S(1)} async-done(((bf16[32,4,256]{2,1,0:T(4,128)(2,1)}), bf16[32,4,256]{2,1,0:T(4,128)(2,1)S(1)}, u32[]{:S(2)}, u32[]{:S(2)}) %all-to-all-start.3) | async-done | bytes 65568 | tf_op jit(solution)/shard_map/all_to_all | solution.py:15
  127.2 0.1 fusion.1
  127.3 0.1 copy.78
  127.5 14.1 %all_to_all.45 = bf16[8,128,128]{2,1,0:T(8,128)(2,1)S(1)} all-to-all(bf16[8,128,128]{2,1,0:T(8,128)(2,1)S(1)} %broadcast_in_dim.29), channel_id=1, replica_groups=mesh['grp'=2,'kv'=32,'tp'=8] {'tp'}, dimensions={0} | all-to-all | bytes 524288 | tf_op jit(solution)/shard_map/all_to_all | solution.py:15
  141.7 7.2 %all_to_all.46 = bf16[4,128,128]{2,1,0:T(8,128)(2,1)S(1)} all-to-all(bf16[4,128,128]{2,1,0:T(8,128)(2,1)S(1)} %broadcast_in_dim.31), channel_id=1, replica_groups={{0,8,16,24},{32,40,48,56},{64,72,80,88},{96,104,112,120},{128,136,144,1..., dimensions={0} | all-to-all | bytes 262144 | tf_op jit(solution)/shard_map/all_to_all | solution.py:15
  148.9 0.1 multiply_reduce_fusion.1
  149.0 0.1 fusion.10
  149.2 0.3 fusion
  149.5 32.3 %all_to_all.47 = bf16[8,16,768]{2,1,0:T(8,128)(2,1)S(1)} all-to-all(bf16[8,16,768]{2,1,0:T(8,128)(2,1)S(1)} %bitcast.89), channel_id=1, replica_groups={{0,32,64,96,128,160,192,224},{8,40,72,104,136,168,200,232},{16,48,80,11..., dimensions={0} | all-to-all | bytes 393216 | tf_op jit(solution)/shard_map/all_to_all | solution.py:15
  181.8 0.2 fusion.27
  182.0 0.1 fusion.24
  182.1 32.5 %all_to_all.48 = bf16[8,16,352]{2,1,0:T(8,128)(2,1)S(1)} all-to-all(bf16[8,16,352]{2,1,0:T(8,128)(2,1)S(1)} %broadcast_in_dim.33), channel_id=1, replica_groups={{0,32,64,96,128,160,192,224},{8,40,72,104,136,168,200,232},{16,48,80,11..., dimensions={0} | all-to-all | bytes 180224 | tf_op jit(solution)/shard_map/all_to_all | solution.py:15
  214.7 0.3 convolution_convert_fusion.1
  215.0 16.9 %all_to_all.49 = bf16[32,16,128]{2,1,0:T(8,128)(2,1)S(1)} all-to-all(bf16[32,16,128]{2,1,0:T(8,128)(2,1)S(1)} %bitcast.93), channel_id=1, replica_groups={{0,1,2,3,4,5,6,7,8,9,10,11,12,13,14,15,16,17,18,19,20,21,22,23,24,25,26..., dimensions={0} | all-to-all | bytes 262144 | tf_op jit(solution)/shard_map/all_to_all | solution.py:15
  232.0 0.6 fusion.29
  (61 shorter events, 0.7 us)
Async XLA Ops:
  0.6 126.5 %copy-start = (bf16[256,128]{1,0:T(8,128)(2,1)S(1)}, bf16[256,128]{1,0:T(8,128)(2,1)}, u32[]{:S(2)}) copy-start(bf16[256,128]{1,0:T(8,128)(2,1)} %param.23) | copy-start | bytes 196612
  0.6 48.3 %copy-start.4 = (bf16[128,1408]{1,0:T(8,128)(2,1)S(1)}, bf16[128,1408]{1,0:T(8,128)(2,1)}, u32[]{:S(2)}) copy-start(bf16[128,1408]{1,0:T(8,128)(2,1)} %param.25) | copy-start | bytes 1081348
  2.0 49.5 %all-to-all-start = ((bf16[8,16,128]{2,1,0:T(8,128)(2,1)}), bf16[8,16,128]{2,1,0:T(8,128)(2,1)S(1)}, u32[]{:S(2)}, u32[]{:S(2)}) async-start(bf16[8,16,128]{2,1,0:T(8,128)(2,1)} %broadcast_in_dim.24), calls=%async_computation | async-start | bytes 65536 | tf_op jit(solution)/shard_map/all_to_all | solution.py:15
  46.7 2.6 %copy-start.6 = (bf16[128,256]{1,0:T(8,128)(2,1)S(1)}, bf16[128,256]{1,0:T(8,128)(2,1)}, u32[]{:S(2)}) copy-start(bf16[128,256]{1,0:T(8,128)(2,1)} %param.19) | copy-start | bytes 196612
  46.7 2.6 %copy-start.7 = (bf16[128,256]{1,0:T(8,128)(2,1)S(1)}, bf16[128,256]{1,0:T(8,128)(2,1)}, u32[]{:S(2)}) copy-start(bf16[128,256]{1,0:T(8,128)(2,1)} %param.18) | copy-start | bytes 196612
  46.7 2.6 %copy-start.8 = (bf16[128,256]{1,0:T(8,128)(2,1)S(1)}, bf16[128,256]{1,0:T(8,128)(2,1)}, u32[]{:S(2)}) copy-start(bf16[128,256]{1,0:T(8,128)(2,1)} %param.17) | copy-start | bytes 196612
  46.7 2.6 %copy-start.9 = (bf16[128,256]{1,0:T(8,128)(2,1)S(1)}, bf16[128,256]{1,0:T(8,128)(2,1)}, u32[]{:S(2)}) copy-start(bf16[128,256]{1,0:T(8,128)(2,1)} %param.16) | copy-start | bytes 196612
  48.9 0.7 copy-start.12
  48.9 0.7 copy-start.13
  52.0 4.7 %copy-start.3 = (bf16[128,1408]{1,0:T(8,128)(2,1)S(1)}, bf16[128,1408]{1,0:T(8,128)(2,1)}, u32[]{:S(2)}) copy-start(bf16[128,1408]{1,0:T(8,128)(2,1)} %param.26) | copy-start | bytes 1081348
  52.9 4.5 %copy-start.5 = (bf16[1408,128]{1,0:T(8,128)(2,1)S(1)}, bf16[1408,128]{1,0:T(8,128)(2,1)}, u32[]{:S(2)}) copy-start(bf16[1408,128]{1,0:T(8,128)(2,1)} %param.27) | copy-start | bytes 1081348
  52.9 11.7 %all-to-all-start.1 = ((bf16[4,8,4,1152]{3,2,1,0:T(4,128)(2,1)}), bf16[4,8,4,1152]{3,2,1,0:T(4,128)(2,1)S(1)}, u32[]{:S(2)}, u32[]{:S(2)}) async-start(bf16[4,8,4,1152]{3,2,1,0:T(4,128)(2,1)} %bitcast.81), calls=%async_computation.1 | async-start | bytes 589824 | tf_op jit(solution)/shard_map/all_to_all | solution.py:15
  56.6 0.9 copy-start.11
  57.5 14.3 %copy-start.10 = (f32[256]{0:T(256)S(1)}, f32[256]{0:T(256)}, u32[]{:S(2)}) copy-start(f32[256]{0:T(256)} %param.20) | copy-start | bytes 3076
  65.3 28.5 %all-to-all-start.2 = ((bf16[8,4,1152]{2,1,0:T(4,128)(2,1)}), bf16[8,4,1152]{2,1,0:T(4,128)(2,1)S(1)}, u32[]{:S(2)}, u32[]{:S(2)}) async-start(bf16[8,4,1152]{2,1,0:T(4,128)(2,1)} %reduce_sum.96), calls=%async_computation.2 | async-start | bytes 147456 | tf_op jit(solution)/shard_map/all_to_all | solution.py:15
  71.9 22.4 %copy-start.2 = (f32[4,2,128,128]{3,2,1,0:T(8,128)S(1)}, f32[4,2,128,128]{3,2,1,0:T(8,128)}, u32[]{:S(2)}) copy-start(f32[4,2,128,128]{3,2,1,0:T(8,128)} %param.21) | copy-start | bytes 1572868
  72.0 32.5 %collective-permute-start = (bf16[1072,128]{1,0:T(8,128)(2,1)S(1)}, bf16[1072,128]{1,0:T(8,128)(2,1)S(1)}, u32[]{:S(2)}, u32[]{:S(2)}) collective-permute-start(bf16[1072,128]{1,0:T(8,128)(2,1)S(1)} %get-tuple-element.58), channel_id=1, source_target_pairs={{0,8},{8,0},{16,24},{24,16},{32,40},{40,32},{48,56},{56,48},{64,72... | collective-permute-start | bytes 823304 | tf_op jit(solution)/shard_map/ppermute | solution.py:41
  74.1 30.4 %collective-permute-start.2 = (bf16[1072,128]{1,0:T(8,128)(2,1)S(1)}, bf16[1072,128]{1,0:T(8,128)(2,1)S(1)}, u32[]{:S(2)}, u32[]{:S(2)}) collective-permute-start(bf16[1072,128]{1,0:T(8,128)(2,1)S(1)} %get-tuple-element.59), channel_id=1, source_target_pairs={{0,24},{8,16},{16,8},{24,0},{32,56},{40,48},{48,40},{56,32},{64,88... | collective-permute-start | bytes 823304 | tf_op jit(solution)/shard_map/ppermute | solution.py:41
  78.1 27.2 %collective-permute-start.1 = (bf16[1072,128]{1,0:T(8,128)(2,1)S(1)}, bf16[1072,128]{1,0:T(8,128)(2,1)S(1)}, u32[]{:S(2)}, u32[]{:S(2)}) collective-permute-start(bf16[1072,128]{1,0:T(8,128)(2,1)S(1)} %get-tuple-element.60), channel_id=1, source_target_pairs={{0,16},{8,24},{16,0},{24,8},{32,48},{40,56},{48,32},{56,40},{64,80... | collective-permute-start | bytes 823304 | tf_op jit(solution)/shard_map/ppermute | solution.py:41
  95.4 31.7 %all-to-all-start.3 = ((bf16[32,4,256]{2,1,0:T(4,128)(2,1)}), bf16[32,4,256]{2,1,0:T(4,128)(2,1)S(1)}, u32[]{:S(2)}, u32[]{:S(2)}) async-start(bf16[32,4,256]{2,1,0:T(4,128)(2,1)} %broadcast_in_dim.27), calls=%async_computation.3 | async-start | bytes 131072 | tf_op jit(solution)/shard_map/all_to_all | solution.py:15
  105.7 1.0 copy-start.1
  149.2 65.5 %slice-start = ((bf16[4,1072,128]{2,1,0:T(8,128)(2,1)}), bf16[4,352,128]{2,1,0:T(8,128)(2,1)S(1)}, s32[]{:S(2)}) async-start(bf16[4,1072,128]{2,1,0:T(8,128)(2,1)} %copy-done.1), calls=%async_computation.9 | async-start | bytes 720896 | tf_op jit(solution)/shard_map/slice | solution.py:141
